TPU v7x, 256 devices: a whole 4x4x8 slice. The times are simulated.
256 devices in a mesh: ep: 16 (over y, x), tp: 16 (over z, core).
Axes of the slice: x: 4, y: 4, z: 8, core: 2. Of those that a mesh axis runs over, the one named last changes fastest.
Arguments:
- queries: bfloat16 [16384, 1024], P('ep', 'tp'), may hold values from -30 to 30
- key_vectors: bfloat16 [16384, 1024], P('ep', 'tp'), may hold values from -30 to 30
- value_vectors: bfloat16 [16384, 1024], P('ep', 'tp'), may hold values from -9 to 9
- cumulative_gate: float32 [16384, 16], P('ep', 'tp'), as said below
- out_weight: bfloat16 [1024, 2048], P('tp'), may hold values from -0.1875 to 0.1875
- expert_tokens: bfloat16 [24576, 2048], P(('ep', 'tp')), may hold values from -6 to 6
- norm_gain: float32 [2048], replicated, may hold values from 0.1 to 1.9
- gate_weight: bfloat16 [16, 2048, 2048], P('ep', None, 'tp'), may hold values from -0.375 to 0.375
- up_weight: bfloat16 [16, 2048, 2048], P('ep', None, 'tp'), may hold values from -0.375 to 0.375
- down_weight: bfloat16 [16, 2048, 2048], P('ep', 'tp'), may hold values from -0.015625 to 0.015625
- expert_choice: int32 [24576, 2], P(('ep', 'tp')), may hold values from 0 to 15, all different within a row; in each aligned block of 96 rows (0 to 95, 96 to 191, ...) at most 13 rows name the same one
- route_weights: float32 [24576, 2], P(('ep', 'tp')), may hold values from 0.2 to 1
Outputs:
- mixer_output: bfloat16 [16384, 2048], P(('ep', 'tp'))
- expert_output: bfloat16 [24576, 2048], P(('ep', 'tp'))
Inputs may be any that keep to these rules, and one draw needn't show every extreme that they name: `cumulative_gate`: each head's values never rise from one position to the next. `expert_choice`: each row names 2 different experts; within the rows of one device no expert is named more than 13 times, and in some of them one expert exactly 13 times.
All inputs are finite; a program needn't handle non-finite values.
Results may differ from a plain program's by a relative error of at most 0.019.
Values may be sent and summed in bfloat16 or wider, within the bound.
No kernel may reach another device: no remote copies, remote signals or barrier semaphores. Data moves between devices by JAX's collectives and lax.ppermute only.
A program may use at most 128 MiB of HBM per device.

v0:
```python
import jax
import jax.numpy as jnp
from jax import lax
from jax.experimental import pallas as pl
from jax.experimental.pallas import tpu as pltpu
from jax.sharding import PartitionSpec as P

EXPERTS = 16
PAD = 16
BLOCK = 1024
HEAD = 64
EPS = 1e-05
CLAMP = 7.0
ALPHA = 1.702
TILE = 256
NEG = float("-inf")
F32 = jnp.float32
BF16 = jnp.bfloat16


def whole(shape):
    return pl.BlockSpec(shape, lambda *_: (0,) * len(shape))


def params(limit=16 << 20):
    return pltpu.CompilerParams(vmem_limit_bytes=limit)


def slots_of(choice):
    rows = choice.shape[0]
    first, second = choice[:, 0:1], choice[:, 1:2]
    lane = lax.broadcasted_iota(jnp.int32, (rows, 128), 1)
    pick0 = (lane == first).astype(F32)
    pick1 = (lane == second).astype(F32)
    below = (
        lax.broadcasted_iota(jnp.int32, (rows, rows), 1)
        < lax.broadcasted_iota(jnp.int32, (rows, rows), 0)
    ).astype(F32)
    before = jnp.dot(
        below.astype(BF16), (pick0 + pick1).astype(BF16), preferred_element_type=F32
    )
    rank0 = jnp.sum(before * pick0, axis=1, keepdims=True).astype(jnp.int32)
    rank1 = jnp.sum(before * pick1, axis=1, keepdims=True).astype(jnp.int32)
    return first * PAD + rank0, second * PAD + rank1


def dispatch_body(tokens_ref, gain_ref, choice_ref, out_ref):
    x = tokens_ref[...].astype(F32)
    scale = lax.rsqrt(jnp.mean(x * x, axis=1, keepdims=True) + EPS)
    normed = (x * scale * gain_ref[...]).astype(BF16)
    slot0, slot1 = slots_of(choice_ref[...])
    lane = lax.broadcasted_iota(jnp.int32, (x.shape[0], EXPERTS * PAD), 1)
    placing = jnp.where((lane == slot0) | (lane == slot1), 1.0, 0.0).astype(BF16)
    out_ref[...] = lax.dot_general(
        placing, normed, (((0,), (0,)), ((), ())), preferred_element_type=F32
    ).astype(BF16)


def dispatch(tokens, gain, choice):
    return pl.pallas_call(
        dispatch_body,
        out_shape=jax.ShapeDtypeStruct((EXPERTS * PAD, tokens.shape[1]), BF16),
        compiler_params=params(),
        name="dispatch",
    )(tokens, gain, choice)


def combine_body(own_ref, choice_ref, weight_ref, out_ref):
    slot0, slot1 = slots_of(choice_ref[...])
    w = weight_ref[...]
    lane = lax.broadcasted_iota(jnp.int32, (w.shape[0], EXPERTS * PAD), 1)
    mix = jnp.where(lane == slot0, w[:, 0:1], 0.0) + jnp.where(lane == slot1, w[:, 1:2], 0.0)
    high = mix.astype(BF16)
    low = (mix - high.astype(F32)).astype(BF16)
    rows = own_ref[...]
    out_ref[...] = (
        jnp.dot(high, rows, preferred_element_type=F32)
        + jnp.dot(low, rows, preferred_element_type=F32)
    ).astype(BF16)


def combine(returned, choice, weights):
    return pl.pallas_call(
        combine_body,
        out_shape=jax.ShapeDtypeStruct((choice.shape[0], returned.shape[1]), BF16),
        compiler_params=params(),
        name="combine",
    )(returned, choice, weights)


def gated(gate_pre, up_pre):
    g = jnp.minimum(gate_pre, CLAMP)
    u = jnp.clip(up_pre, -CLAMP, CLAMP)
    return (g * jax.nn.sigmoid(ALPHA * g) * (u + 1.0)).astype(BF16)


def nt(a, b):
    return lax.dot_general(a, b, (((1,), (1,)), ((), ())), preferred_element_type=F32)


def hidden(rows, gu_refs):
    acts = []
    for gu in gu_refs:
        pre = jnp.dot(
            rows, jnp.concatenate([gu[0], gu[1]], axis=1), preferred_element_type=F32
        )
        acts.append(gated(pre[:, :128], pre[:, 128:]))
    return jnp.concatenate(acts, axis=1) if len(acts) > 1 else acts[0]


def stacked(d_refs):
    downs = [d[...] for d in d_refs]
    return jnp.concatenate(downs, axis=0) if len(downs) > 1 else downs[0]


def experts(x, gus, downs, y, first=0, count=None, keep=True):
    d = x.shape[1]
    n = len(gus)
    count = x.shape[0] // 256 if count is None else count

    def body(*refs):
        x_ref, gu_refs, d_refs, out_ref = refs[0], refs[1 : 1 + n], refs[1 + n : 1 + 2 * n], refs[-1]
        total = jnp.dot(
            hidden(x_ref[...], gu_refs), stacked(d_refs), preferred_element_type=F32
        )
        if y is not None:
            total = total + refs[-2][...].astype(F32)
        out_ref[...] = total.astype(BF16)

    rows = pl.BlockSpec((256, d), lambda i: (i + first, 0))
    args = [x, *gus, *downs] + ([] if y is None else [y])
    specs = [rows] + [whole(w.shape) for w in (*gus, *downs)] + ([] if y is None else [rows])
    return pl.pallas_call(
        body,
        grid=(count,),
        in_specs=specs,
        out_specs=pl.BlockSpec((256, d), lambda i: (i, 0)),
        out_shape=pltpu.HBM((count * 256, d), BF16) if keep else jax.ShapeDtypeStruct((count * 256, d), BF16),
        compiler_params=params(),
        name="experts",
        cost_estimate=pl.CostEstimate(
            flops=6 * count * 256 * d * 128 * n,
            transcendentals=count * 256 * 128,
            bytes_accessed=6 << 20,
        ),
    )(*args)


def attend(ep, base, q, kvg, state, first, last, finish):
    tiles = BLOCK // TILE

    def body(ep_ref, base_ref, q_ref, kv_ref, *rest):
        if state is not None:
            m_in, acc_in = rest[0], rest[1]
            rest = rest[2:]
        if finish:
            out_ref, m_ref, acc_ref = rest
        else:
            m_ref, acc_ref = rest
        if state is None:
            m_ref[...] = jnp.full(m_ref.shape, NEG, F32)
            acc_ref[...] = jnp.zeros(acc_ref.shape, F32)
        else:
            m_ref[...] = m_in[...]
            acc_ref[...] = acc_in[...]
        me = ep_ref[0]
        base = base_ref[...]
        lane = lax.broadcasted_iota(jnp.int32, (BLOCK, 128), 1)

        def one(j, masked):
            kv = kv_ref[j, 0:BLOCK, :]
            parts = kv_ref[j, BLOCK : BLOCK + 32, :].astype(F32)
            gates = (parts[0:8] + parts[8:16]) + parts[16:24]
            decay = base - gates
            row = jnp.concatenate([decay[c : c + 1] for c in range(8)], axis=1)
            values = jnp.where(lane < HEAD, jnp.ones_like(kv), kv)

            def scores(t):
                return nt(q_ref[t * TILE : (t + 1) * TILE, :], kv)

            ahead = scores(0)
            for t in range(tiles):
                s = ahead
                if t + 1 < tiles:
                    ahead = scores(t + 1)
                at = slice(t * TILE, (t + 1) * TILE)
                s = s + row
                if masked:
                    qpos = t * TILE + lax.broadcasted_iota(jnp.int32, (TILE, BLOCK), 0)
                    kpos = lax.broadcasted_iota(jnp.int32, (TILE, BLOCK), 1)
                    s = jnp.where(kpos <= qpos, s, NEG)
                old = m_ref[at, :]
                peak = jnp.maximum(
                    old, jnp.broadcast_to(jnp.max(s, axis=1, keepdims=True), (TILE, 128))
                )
                weight = jnp.exp(s - jnp.concatenate([peak] * (BLOCK // 128), axis=1))
                acc_ref[at, :] = acc_ref[at, :] * jnp.exp(old - peak) + jnp.dot(
                    weight.astype(BF16), values, preferred_element_type=F32
                )
                m_ref[at, :] = peak

        def step(j, carry):
            one(j - first, False)
            return carry

        lax.fori_loop(first, jnp.minimum(me, last), step, 0)

        @pl.when((me >= first) & (me < last))
        def _():
            one(me - first, True)

        if finish:
            for g in range(BLOCK // 64):
                a = acc_ref[64 * g : 64 * g + 32, :]
                b = acc_ref[64 * g + 32 : 64 * g + 64, :]
                pair = [a[:, HEAD:] / a[:, :HEAD], b[:, HEAD:] / b[:, :HEAD]]
                out_ref[32 * g : 32 * g + 32, :] = jnp.concatenate(pair, axis=1).astype(BF16)

    span = last - first
    args = [ep, base, q, kvg]
    specs = [
        pl.BlockSpec(memory_space=pltpu.SMEM),
        whole(base.shape),
        whole(q.shape),
        pl.BlockSpec((span,) + kvg.shape[1:], lambda *_: (first // span, 0, 0)),
    ]
    wide = jax.ShapeDtypeStruct((BLOCK, 128), F32)
    if state is not None:
        args += list(state)
        specs += [whole(wide.shape)] * 2
    if finish:
        outs = jax.ShapeDtypeStruct((BLOCK // 2, 2 * HEAD), BF16)
        out_specs = whole(outs.shape)
        scratch = [pltpu.VMEM(wide.shape, F32)] * 2
    else:
        outs = (wide, wide)
        out_specs = (whole(wide.shape),) * 2
        scratch = []
    return pl.pallas_call(
        body,
        grid=(1,),
        in_specs=specs,
        out_specs=out_specs,
        out_shape=outs,
        scratch_shapes=scratch,
        compiler_params=params(),
        name="attend",
        cost_estimate=pl.CostEstimate(
            flops=span * BLOCK * BLOCK * 1024, transcendentals=0, bytes_accessed=4 << 20
        ),
    )(*args)


def arrange(place, near):
    n = len(near)

    def body(place_ref, *refs):
        out_ref = refs[-1]
        chip = lax.div(place_ref[0], 2)
        core = lax.rem(place_ref[0], 2)
        for s in range(n):
            at = lax.rem(chip + s, n) * 2 * HEAD
            mine = pl.multiple_of(at + core * HEAD, HEAD)
            other = pl.multiple_of(at + (1 - core) * HEAD, HEAD)
            out_ref[pl.ds(mine, HEAD), :] = refs[s][:HEAD, :]
            out_ref[pl.ds(other, HEAD), :] = refs[s][HEAD:, :]

    return pl.pallas_call(
        body,
        grid=(1,),
        in_specs=[pl.BlockSpec(memory_space=pltpu.SMEM)] + [whole(a.shape) for a in near],
        out_specs=whole((n * 2 * HEAD, 128)),
        out_shape=jax.ShapeDtypeStruct((n * 2 * HEAD, 128), BF16),
        compiler_params=params(),
        name="arrange",
    )(place, *near)


def project(packed, columns):
    heads, half, _ = packed.shape
    width = heads * HEAD

    def body(a_ref, w_ref, out_ref, rows_ref):
        @pl.when(pl.program_id(0) == 0)
        def _():
            for h in range(0, heads, 2):
                a, b = a_ref[h].astype(F32), a_ref[h + 1].astype(F32)
                at = slice(h * HEAD, (h + 2) * HEAD)
                top = jnp.concatenate([a[:, :HEAD], b[:, :HEAD]], axis=1)
                low = jnp.concatenate([a[:, HEAD:], b[:, HEAD:]], axis=1)
                rows_ref[:half, at] = top.astype(BF16)
                rows_ref[half:, at] = low.astype(BF16)

        both = jnp.concatenate([w_ref[0], w_ref[1]], axis=1)
        out_ref[...] = jnp.dot(rows_ref[...], both, preferred_element_type=F32).astype(BF16)

    return pl.pallas_call(
        body,
        grid=(columns.shape[0] // 2,),
        in_specs=[whole(packed.shape), pl.BlockSpec((2, width, 128), lambda i: (i, 0, 0))],
        out_specs=pl.BlockSpec((2 * half, 256), lambda i: (0, i)),
        out_shape=jax.ShapeDtypeStruct((2 * half, columns.shape[0] * 128), BF16),
        scratch_shapes=[pltpu.VMEM((2 * half, width), BF16)],
        compiler_params=params(),
        name="project",
    )(packed, columns)


def local(
    queries,
    key_vectors,
    value_vectors,
    cumulative_gate,
    out_weight,
    expert_tokens,
    norm_gain,
    gate_weight,
    up_weight,
    down_weight,
    expert_choice,
    route_weights,
):
    n_tp = lax.axis_size("tp")
    n_ep = lax.axis_size("ep")
    chips = n_tp // 2
    d = expert_tokens.shape[1]
    spot = [(z, c) for z in range(chips) for c in range(2)]
    ahead = [(2 * z + c, 2 * ((z + 1 - 2 * c) % chips) + c) for z, c in spot]
    back = [(2 * z + c, 2 * ((z - 1 + 2 * c) % chips) + c) for z, c in spot]
    swap = [(2 * z + c, 2 * z + 1 - c) for z, c in spot]
    fence = lax.optimization_barrier

    def ring(a, b):
        return lax.ppermute(a, "tp", ahead), lax.ppermute(b, "tp", back)

    down = down_weight[0]
    da1, db1 = ring(down, down)
    gu = jnp.concatenate([gate_weight, up_weight], axis=0)
    ga1, gb1 = ring(gu, gu)

    high = lax.reduce_precision(cumulative_gate, 8, 7)
    mid = lax.reduce_precision(cumulative_gate - high, 8, 7)
    low = cumulative_gate - high - mid
    gates = jnp.concatenate([high, mid, low, jnp.zeros_like(low)], axis=1)
    gates = gates.T.reshape(32, 128).astype(BF16)
    packed = jnp.concatenate(
        [jnp.concatenate([key_vectors, value_vectors], axis=1), gates], axis=0
    )
    gain = norm_gain[None, :]
    outgoing = dispatch(expert_tokens, gain, expert_choice).reshape(n_ep, PAD, d)
    kvg = lax.all_gather(packed, "ep", axis=0)
    arrived = lax.all_to_all(outgoing, "ep", split_axis=0, concat_axis=0, tiled=True)
    ep = lax.axis_index("ep").astype(jnp.int32).reshape(1)
    q = jnp.concatenate([queries * BF16(0.125), jnp.zeros_like(queries)], axis=1)
    base = jnp.broadcast_to(cumulative_gate[0:1, :], (1, 128))
    strip = lax.dynamic_slice_in_dim(out_weight, lax.axis_index("ep") * 128, 128, 1)
    strip = jnp.concatenate([strip, lax.ppermute(strip, "tp", swap)], axis=0)
    da1, db1, strip = fence((da1, db1, strip))

    da2, db2 = ring(da1, db1)
    near = [strip] + [
        lax.ppermute(
            strip, "tp", [(2 * z + c, 2 * ((z - s) % chips) + c) for z, c in spot]
        )
        for s in range(1, chips)
    ]
    strips = arrange(lax.axis_index("tp").astype(jnp.int32).reshape(1), near)
    ga1, gb1, q, base = fence((ga1, gb1, q, base))

    ga2, gb2 = ring(ga1, gb1)
    columns = lax.all_gather(strips, "ep", axis=0)
    arrived = arrived.reshape(n_ep * PAD, d)
    beside = lax.ppermute(arrived, "tp", swap)
    x = jnp.concatenate([arrived, beside], axis=0)
    y = experts(x, [gu, ga1], [down, da1], None)
    da2, db2, y = fence((da2, db2, y))

    da3, db3 = ring(da2, db2)
    half = n_ep // 2
    y = experts(x, [gb1], [db1], y)
    state = attend(ep, base, q, kvg, None, 0, half, False)
    ga2, gb2, y, state = fence((ga2, gb2, y, state))

    ga3, gb3 = ring(ga2, gb2)
    attention = attend(ep, base, q, kvg, state, half, n_ep, True)
    da3, db3, attention = fence((da3, db3, attention))

    d4 = lax.ppermute(db3, "tp", back)
    y = experts(x, [ga2, gb2], [da2, db2], y)
    ga3, gb3, y, attention = fence((ga3, gb3, y, attention))
    rows = lax.all_to_all(
        attention.reshape(n_tp, -1, 2 * HEAD), "tp", split_axis=0, concat_axis=0, tiled=True
    )

    g4 = lax.ppermute(ga3, "tp", ahead)
    y = experts(x, [ga3, gb3], [da3, db3], y)
    g4, d4, y, rows = fence((g4, d4, y, rows))

    theirs = experts(x, [g4], [d4], y, 1, 1, False)
    extra = lax.ppermute(theirs, "tp", swap)
    mine = experts(x, [g4], [d4], y, 0, 1, False)
    results = (mine.astype(F32) + extra.astype(F32)).astype(BF16).reshape(n_ep, PAD, d)
    returned = lax.all_to_all(results, "ep", split_axis=0, concat_axis=0, tiled=True)
    rows, results = fence((rows, results))
    mixer_output = project(rows, columns)
    expert_output = combine(returned.reshape(n_ep * PAD, d), expert_choice, route_weights)
    return (mixer_output, expert_output)


def solution(mesh):
    placed = (
        P("ep", "tp"),
        P("ep", "tp"),
        P("ep", "tp"),
        P("ep", "tp"),
        P("tp", None),
        P(("ep", "tp"), None),
        P(),
        P("ep", None, "tp"),
        P("ep", None, "tp"),
        P("ep", "tp", None),
        P(("ep", "tp"), None),
        P(("ep", "tp"), None),
    )

    return jax.shard_map(
        local,
        mesh=mesh,
        in_specs=placed,
        out_specs=(P(("ep", "tp"), None), P(("ep", "tp"), None)),
        check_vma=False,
    )
```

profile of v0, /device:TPU:2, one launch (start us, length us, event | category | flops | bytes accessed | tf_op | source)
XLA Modules:
  0.0 212.0 jit_solution(14363144662448642977)
XLA Ops:
  8.2 1.1 copy.29
  9.2 1.1 copy.30
  11.2 2.0 collective-permute-start.5
  13.2 4.0 %collective-permute-start.6 = (bf16[128,2048]{1,0:T(8,128)(2,1)}, bf16[128,2048]{1,0:T(8,128)(2,1)}, u32[]{:S(2)}, u32[]{:S(2)}) collective-permute-start(bf16[128,2048]{1,0:T(8,128)(2,1)} %bitcast.18), channel_id=1, source_target_pairs={{0,14},{1,3},{2,0},{3,5},{4,2},{5,7},{6,4},{7,9},{8,6},{9,11},{10,... | collective-permute-start | bytes 1572872 | tf_op jit(solution)/shard_map/ppermute | solution.py:334
  18.9 1.8 dispatch.1
  20.7 7.6 %all-to-all-start = ((bf16[16,16,2048]{2,1,0:T(8,128)(2,1)}), bf16[16,16,2048]{2,1,0:T(8,128)(2,1)S(1)}, u32[]{:S(2)}, u32[]{:S(2)}) async-start(bf16[16,16,2048]{2,1,0:T(8,128)(2,1)} %bitcast.2), calls=%async_computation | async-start | bytes 2097152 | tf_op jit(solution)/shard_map/all_to_all | solution.py:352
  28.6 3.7 %collective-permute-start.17 = (bf16[128,128]{1,0:T(8,128)(2,1)S(1)}, bf16[128,128]{1,0:T(8,128)(2,1)S(1)}, u32[]{:S(2)}, u32[]{:S(2)}) collective-permute-start(bf16[128,128]{1,0:T(8,128)(2,1)S(1)} %pad_maximum_fusion.2.refs_0_), channel_id=1, source_target_pairs={{0,14},{1,15},{2,0},{3,1},{4,2},{5,3},{6,4},{7,5},{8,6},{9,7},{10,... | collective-permute-start | bytes 98312 | tf_op jit(solution)/shard_map/ppermute | solution.py:362
  32.3 1.0 collective-permute-start.18
  33.3 1.0 collective-permute-start.19
  34.3 4.5 %collective-permute-start.20 = (bf16[128,128]{1,0:T(8,128)(2,1)S(1)}, bf16[128,128]{1,0:T(8,128)(2,1)S(1)}, u32[]{:S(2)}, u32[]{:S(2)}) collective-permute-start(bf16[128,128]{1,0:T(8,128)(2,1)S(1)} %pad_maximum_fusion.2.refs_0_), channel_id=1, source_target_pairs={{0,8},{1,9},{2,10},{3,11},{4,12},{5,13},{6,14},{7,15},{8,0},{9,1},... | collective-permute-start | bytes 98312 | tf_op jit(solution)/shard_map/ppermute | solution.py:362
  38.8 3.1 %collective-permute-start.22 = (bf16[128,128]{1,0:T(8,128)(2,1)S(1)}, bf16[128,128]{1,0:T(8,128)(2,1)S(1)}, u32[]{:S(2)}, u32[]{:S(2)}) collective-permute-start(bf16[128,128]{1,0:T(8,128)(2,1)S(1)} %pad_maximum_fusion.2.refs_0_), channel_id=1, source_target_pairs={{0,4},{1,5},{2,6},{3,7},{4,8},{5,9},{6,10},{7,11},{8,12},{9,13},{1... | collective-permute-start | bytes 98312 | tf_op jit(solution)/shard_map/ppermute | solution.py:362
  41.9 1.8 collective-permute-start.23
  43.8 2.2 %collective-permute-done.21.refs_5_ = bf16[128,128]{1,0:T(8,128)(2,1)S(1)} collective-permute-done((bf16[128,128]{1,0:T(8,128)(2,1)S(1)}, bf16[128,128]{1,0:T(8,128)(2,1)S(1)}, u32[]{:S(2)}, u32[]{:S(2)}) %collective-permute-start.21) | collective-permute-done | bytes 32800 | tf_op jit(solution)/shard_map/ppermute | solution.py:362
  45.9 1.0 collective-permute-done.22.refs_6_
  48.0 1.1 constant_dynamic-update-slice_fusion.refs_1_
  50.0 2.5 %collective-permute-start.1 = (bf16[2,2048,128]{2,1,0:T(8,128)(2,1)S(1)}, bf16[2,2048,128]{2,1,0:T(8,128)(2,1)}, u32[]{:S(2)}, u32[]{:S(2)}) collective-permute-start(bf16[2,2048,128]{2,1,0:T(8,128)(2,1)S(1)} %constant_dynamic-update-slice_fusion.refs_1_), channel_id=1, source_target_pairs={{0,14},{1,3},{2,0},{3,5},{4,2},{5,7},{6,4},{7,9},{8,6},{9,11},{10,... | collective-permute-start | bytes 3145736 | tf_op jit(solution)/shard_map/ppermute | solution.py:334
  52.8 3.2 %collective-permute-start.9 = (bf16[128,2048]{1,0:T(8,128)(2,1)}, bf16[128,2048]{1,0:T(8,128)(2,1)S(1)}, u32[]{:S(2)}, u32[]{:S(2)}) collective-permute-start(bf16[128,2048]{1,0:T(8,128)(2,1)} %collective-permute-done.6.refs_2_), channel_id=1, source_target_pairs={{0,14},{1,3},{2,0},{3,5},{4,2},{5,7},{6,4},{7,9},{8,6},{9,11},{10,... | collective-permute-start | bytes 1572872 | tf_op jit(solution)/shard_map/ppermute | solution.py:334
  56.0 1.1 slice.3
  57.9 18.7 %collective-permute-done.refs_2_ = bf16[2,2048,128]{2,1,0:T(8,128)(2,1)} collective-permute-done((bf16[2,2048,128]{2,1,0:T(8,128)(2,1)S(1)}, bf16[2,2048,128]{2,1,0:T(8,128)(2,1)}, u32[]{:S(2)}, u32[]{:S(2)}) %collective-permute-start) | collective-permute-done | bytes 1048608 | tf_op jit(solution)/shard_map/ppermute | solution.py:334
  77.2 3.3 %collective-permute-start.3 = (bf16[2,2048,128]{2,1,0:T(8,128)(2,1)}, bf16[2,2048,128]{2,1,0:T(8,128)(2,1)}, u32[]{:S(2)}, u32[]{:S(2)}) collective-permute-start(bf16[2,2048,128]{2,1,0:T(8,128)(2,1)} %collective-permute-done.1.refs_1_), channel_id=1, source_target_pairs={{0,14},{1,3},{2,0},{3,5},{4,2},{5,7},{6,4},{7,9},{8,6},{9,11},{10,... | collective-permute-start | bytes 3145736 | tf_op jit(solution)/shard_map/ppermute | solution.py:334
  80.6 1.7 pad_maximum_fusion.refs_0_
  82.2 4.5 %experts.6.refs_3_ = bf16[512,2048]{1,0:T(8,128)(2,1)} custom-call(bf16[512,2048]{1,0:T(8,128)(2,1)S(1)} %pad_maximum_fusion.refs_0_, bf16[2,2048,128]{2,1,0:T(8,128)(2,1)S(1)} %constant_dynamic-update-slice_fusion.refs_1_, bf16[2,2048,128]{2,1,0:T(8,128)(2,1)} %collective-permute-done.refs_2_, bf16[128,2048]{1,0:T(8,128)(2,1)S(1)} %bitcast.19, ...), custom_call_target="tpu_custom_call" | custom-call | flops 1610612736 | bytes 6291456 | tf_op jit(solution)/shard_map/experts/pallas_call | solution.py:133
  89.3 1.6 copy-done.2
  90.9 5.0 %experts.7.refs_5_ = bf16[512,2048]{1,0:T(8,128)(2,1)} custom-call(bf16[512,2048]{1,0:T(8,128)(2,1)S(1)} %pad_maximum_fusion.refs_0_, bf16[2,2048,128]{2,1,0:T(8,128)(2,1)} %collective-permute-done.1.refs_1_, bf16[128,2048]{1,0:T(8,128)(2,1)} %collective-permute-done.6.refs_2_, bf16[512,2048]{1,0:T(8,128)(2,1)S(1)} %copy-done.2), custom_call_target="tpu_custom_call" | custom-call | flops 805306368 | bytes 6291456 | tf_op jit(solution)/shard_map/experts/pallas_call | solution.py:133
  95.9 2.3 %copy-done.21 = bf16[16896,128]{1,0:T(8,128)(2,1)S(1)} copy-done((bf16[16896,128]{1,0:T(8,128)(2,1)S(1)}, bf16[16896,128]{1,0:T(8,128)(2,1)}, u32[]{:S(2)}) %copy-start.21) | copy-done | bytes 4325400
  98.2 3.9 %attend.2 = (f32[1024,128]{1,0:T(8,128)S(1)}, f32[1024,128]{1,0:T(8,128)S(1)}) custom-call(s32[1]{0:T(128)} %bitcast.5.ep_ref, f32[1,128]{1,0:T(1,128)S(1)} %broadcast_in_dim.15.base_ref, bf16[1024,128]{1,0:T(8,128)(2,1)S(1)} %copy-done.18, bf16[16,1056,128]{2,1,0:T(8,128)(2,1)S(1)} %bitcast.22), custom_call_target="tpu_custom_call" | custom-call | flops 8589934592 | bytes 4194304 | tf_op jit(solution)/shard_map/attend/pallas_call | solution.py:239
  102.1 5.3 %collective-permute-done.2.refs_1_ = bf16[2,2048,128]{2,1,0:T(8,128)(2,1)} collective-permute-done((bf16[2,2048,128]{2,1,0:T(8,128)(2,1)}, bf16[2,2048,128]{2,1,0:T(8,128)(2,1)}, u32[]{:S(2)}, u32[]{:S(2)}) %collective-permute-start.2) | collective-permute-done | bytes 1048608 | tf_op jit(solution)/shard_map/ppermute | solution.py:334
  107.6 3.0 %collective-permute-start.11 = (bf16[2,2048,128]{2,1,0:T(8,128)(2,1)}, bf16[2,2048,128]{2,1,0:T(8,128)(2,1)S(1)}, u32[]{:S(2)}, u32[]{:S(2)}) collective-permute-start(bf16[2,2048,128]{2,1,0:T(8,128)(2,1)} %collective-permute-done.3.refs_2_), channel_id=1, source_target_pairs={{0,14},{1,3},{2,0},{3,5},{4,2},{5,7},{6,4},{7,9},{8,6},{9,11},{10,... | collective-permute-start | bytes 3145736 | tf_op jit(solution)/shard_map/ppermute | solution.py:334
  110.6 3.2 %collective-permute-start.13 = (bf16[128,2048]{1,0:T(8,128)(2,1)S(1)}, bf16[128,2048]{1,0:T(8,128)(2,1)}, u32[]{:S(2)}, u32[]{:S(2)}) collective-permute-start(bf16[128,2048]{1,0:T(8,128)(2,1)S(1)} %copy-done.12), channel_id=1, source_target_pairs={{0,14},{1,3},{2,0},{3,5},{4,2},{5,7},{6,4},{7,9},{8,6},{9,11},{10,... | collective-permute-start | bytes 1572872 | tf_op jit(solution)/shard_map/ppermute | solution.py:334
  114.7 28.9 %collective-permute-done.12.refs_3_ = bf16[128,2048]{1,0:T(8,128)(2,1)S(1)} collective-permute-done((bf16[128,2048]{1,0:T(8,128)(2,1)S(1)}, bf16[128,2048]{1,0:T(8,128)(2,1)S(1)}, u32[]{:S(2)}, u32[]{:S(2)}) %collective-permute-start.12) | collective-permute-done | bytes 524320 | tf_op jit(solution)/shard_map/ppermute | solution.py:334
  143.6 4.9 %experts.8.refs_5_ = bf16[512,2048]{1,0:T(8,128)(2,1)} custom-call(bf16[512,2048]{1,0:T(8,128)(2,1)S(1)} %pad_maximum_fusion.refs_0_, bf16[2,2048,128]{2,1,0:T(8,128)(2,1)} %collective-permute-done.2.refs_1_, bf16[2,2048,128]{2,1,0:T(8,128)(2,1)} %collective-permute-done.3.refs_2_, bf16[128,2048]{1,0:T(8,128)(2,1)S(1)} %copy-done.10, ...), custom_call_target="tpu_custom_call" | custom-call | flops 1610612736 | bytes 6291456 | tf_op jit(solution)/shard_map/experts/pallas_call | solution.py:133
  148.6 1.0 copy-done.6
  149.6 3.2 %collective-permute-start.15 = (bf16[128,2048]{1,0:T(8,128)(2,1)}, bf16[128,2048]{1,0:T(8,128)(2,1)}, u32[]{:S(2)}, u32[]{:S(2)}) collective-permute-start(bf16[128,2048]{1,0:T(8,128)(2,1)} %collective-permute-done.13.refs_4_), channel_id=1, source_target_pairs={{0,14},{1,3},{2,0},{3,5},{4,2},{5,7},{6,4},{7,9},{8,6},{9,11},{10,... | collective-permute-start | bytes 1572872 | tf_op jit(solution)/shard_map/ppermute | solution.py:388
  152.8 4.5 %all-to-all-start.1 = ((bf16[16,32,128]{2,1,0:T(8,128)(2,1)}), bf16[16,32,128]{2,1,0:T(8,128)(2,1)S(1)}, u32[]{:S(2)}, u32[]{:S(2)}) async-start(bf16[16,32,128]{2,1,0:T(8,128)(2,1)} %bitcast.20), calls=%async_computation.1 | async-start | bytes 262144 | tf_op jit(solution)/shard_map/all_to_all | solution.py:391
  157.4 1.6 copy-done.4
  158.9 1.2 copy-done.7
  160.2 1.0 copy-done.14
  161.2 4.5 %experts.9.refs_3_ = bf16[512,2048]{1,0:T(8,128)(2,1)} custom-call(bf16[512,2048]{1,0:T(8,128)(2,1)S(1)} %pad_maximum_fusion.refs_0_, bf16[2,2048,128]{2,1,0:T(8,128)(2,1)} %collective-permute-done.10.refs_1_, bf16[2,2048,128]{2,1,0:T(8,128)(2,1)S(1)} %copy-done.7, bf16[128,2048]{1,0:T(8,128)(2,1)S(1)} %copy-done.14, ...), custom_call_target="tpu_custom_call" | custom-call | flops 1610612736 | bytes 6291456 | tf_op jit(solution)/shard_map/experts/pallas_call | solution.py:133
  166.4 6.5 %all-to-all-done.1.a_ref = bf16[16,32,128]{2,1,0:T(8,128)(2,1)S(1)} async-done(((bf16[16,32,128]{2,1,0:T(8,128)(2,1)}), bf16[16,32,128]{2,1,0:T(8,128)(2,1)S(1)}, u32[]{:S(2)}, u32[]{:S(2)}) %all-to-all-start.1) | async-done | bytes 131104 | tf_op jit(solution)/shard_map/all_to_all | solution.py:391
  172.9 1.6 copy-done.1
  174.5 2.3 %experts.11 = bf16[256,2048]{1,0:T(8,128)(2,1)S(1)} custom-call(bf16[512,2048]{1,0:T(8,128)(2,1)S(1)} %pad_maximum_fusion.refs_0_, bf16[2,2048,128]{2,1,0:T(8,128)(2,1)S(1)} %collective-permute-done.14.refs_1_, bf16[128,2048]{1,0:T(8,128)(2,1)} %collective-permute-done.15.refs_2_, bf16[512,2048]{1,0:T(8,128)(2,1)S(1)} %copy-done.1), custom_call_target="tpu_custom_call" | custom-call | flops 402653184 | bytes 6291456 | tf_op jit(solution)/shard_map/experts/pallas_call | solution.py:133
  176.9 2.3 %experts.10 = bf16[256,2048]{1,0:T(8,128)(2,1)S(1)} custom-call(bf16[512,2048]{1,0:T(8,128)(2,1)S(1)} %pad_maximum_fusion.refs_0_, bf16[2,2048,128]{2,1,0:T(8,128)(2,1)S(1)} %collective-permute-done.14.refs_1_, bf16[128,2048]{1,0:T(8,128)(2,1)} %collective-permute-done.15.refs_2_, bf16[512,2048]{1,0:T(8,128)(2,1)S(1)} %copy-done.1), custom_call_target="tpu_custom_call" | custom-call | flops 402653184 | bytes 6291456 | tf_op jit(solution)/shard_map/experts/pallas_call | solution.py:133
  179.6 1.4 add_convert_fusion
  181.0 6.4 %all-to-all-start.2 = ((bf16[16,16,2048]{2,1,0:T(8,128)(2,1)}), bf16[16,16,2048]{2,1,0:T(8,128)(2,1)S(1)}, u32[]{:S(2)}, u32[]{:S(2)}) async-start(bf16[16,16,2048]{2,1,0:T(8,128)(2,1)} %bitcast.9), calls=%async_computation.2 | async-start | bytes 2097152 | tf_op jit(solution)/shard_map/all_to_all | solution.py:403
  187.5 2.2 %copy-done.5 = bf16[16384,128]{1,0:T(8,128)(2,1)S(1)} copy-done((bf16[16384,128]{1,0:T(8,128)(2,1)S(1)}, bf16[16384,128]{1,0:T(8,128)(2,1)}, u32[]{:S(2)}) %copy-start.5) | copy-done | bytes 4194328
  189.7 3.6 %project.1 = bf16[64,2048]{1,0:T(8,128)(2,1)} custom-call(bf16[16,32,128]{2,1,0:T(8,128)(2,1)S(1)} %all-to-all-done.1.a_ref, bf16[16,1024,128]{2,1,0:T(8,128)(2,1)S(1)} %bitcast.15), custom_call_target="tpu_custom_call" | custom-call | tf_op jit(solution)/shard_map/project/pallas_call | solution.py:297
  193.4 10.2 %all-to-all-done.2 = bf16[16,16,2048]{2,1,0:T(8,128)(2,1)S(1)} async-done(((bf16[16,16,2048]{2,1,0:T(8,128)(2,1)}), bf16[16,16,2048]{2,1,0:T(8,128)(2,1)S(1)}, u32[]{:S(2)}, u32[]{:S(2)}) %all-to-all-start.2) | async-done | bytes 1048608 | tf_op jit(solution)/shard_map/all_to_all | solution.py:403
  203.6 1.6 combine.1
  (98 shorter events, 12.3 us)
Async XLA Ops:
  7.2 10.1 %copy-start = (bf16[64,2048]{1,0:T(8,128)(2,1)S(1)}, bf16[64,2048]{1,0:T(8,128)(2,1)}, u32[]{:S(2)}) copy-start(bf16[64,2048]{1,0:T(8,128)(2,1)} %param.16) | copy-start | bytes 786436
  7.2 11.0 %copy-start.17 = (bf16[96,2048]{1,0:T(8,128)(2,1)S(1)}, bf16[96,2048]{1,0:T(8,128)(2,1)}, u32[]{:S(2)}) copy-start(bf16[96,2048]{1,0:T(8,128)(2,1)} %tokens_ref.1) | copy-start | bytes 1179652
  7.2 88.7 %all-gather.5.cloned.1.call-start = ((), (), s32[]{:S(2)}) async-start(), calls=%async_computation.3 | async-start | bytes 4595712 | tf_op jit(solution)/shard_map/all_gather | solution.py:351
  11.2 17.2 %collective-permute-start.5 = (bf16[128,2048]{1,0:T(8,128)(2,1)}, bf16[128,2048]{1,0:T(8,128)(2,1)}, u32[]{:S(2)}, u32[]{:S(2)}) collective-permute-start(bf16[128,2048]{1,0:T(8,128)(2,1)} %bitcast.17), channel_id=1, source_target_pairs={{0,2},{1,15},{2,4},{3,1},{4,6},{5,3},{6,8},{7,5},{8,10},{9,7},{10,... | collective-permute-start | bytes 1572872 | tf_op jit(solution)/shard_map/ppermute | solution.py:334
  13.2 15.4 %collective-permute-start.6 = (bf16[128,2048]{1,0:T(8,128)(2,1)}, bf16[128,2048]{1,0:T(8,128)(2,1)}, u32[]{:S(2)}, u32[]{:S(2)}) collective-permute-start(bf16[128,2048]{1,0:T(8,128)(2,1)} %bitcast.18), channel_id=1, source_target_pairs={{0,14},{1,3},{2,0},{3,5},{4,2},{5,7},{6,4},{7,9},{8,6},{9,11},{10,... | collective-permute-start | bytes 1572872 | tf_op jit(solution)/shard_map/ppermute | solution.py:334
  17.2 11.1 %collective-permute-start.7 = (bf16[64,128]{1,0:T(8,128)(2,1)S(1)}, bf16[64,128]{1,0:T(8,128)(2,1)S(1)}, u32[]{:S(2)}, u32[]{:S(2)}) collective-permute-start(bf16[64,128]{1,0:T(8,128)(2,1)S(1)} %constant_dynamic-slice_fusion), channel_id=1, source_target_pairs={{0,1},{1,0},{2,3},{3,2},{4,5},{5,4},{6,7},{7,6},{8,9},{9,8},{10,11... | collective-permute-start | bytes 49160 | tf_op jit(solution)/shard_map/ppermute | solution.py:357
  18.1 29.8 %copy-start.15 = (s32[96,2]{1,0:T(8,128)}, s32[96,2]{1,0:T(8,128)S(1)}, u32[]{:S(2)}) copy-start(s32[96,2]{1,0:T(8,128)S(1)} %copy.28.choice_ref) | copy-start | bytes 2308
  18.9 29.1 %copy-start.24 = (bf16[1,2048,128]{2,1,0:T(8,128)(2,1)S(1)}, bf16[1,2048,128]{2,1,0:T(8,128)(2,1)}, u32[]{:S(2)}) copy-start(bf16[1,2048,128]{2,1,0:T(8,128)(2,1)} %param.19) | copy-start | bytes 1572868
  20.7 31.8 %copy-start.25 = (bf16[1024,64]{0,1:T(8,128)(2,1)S(1)}, bf16[1024,64]{0,1:T(8,128)(2,1)}, u32[]{:S(2)}) copy-start(bf16[1024,64]{0,1:T(8,128)(2,1)} %param.12) | copy-start | bytes 393220
  20.7 31.8 %all-to-all-start = ((bf16[16,16,2048]{2,1,0:T(8,128)(2,1)}), bf16[16,16,2048]{2,1,0:T(8,128)(2,1)S(1)}, u32[]{:S(2)}, u32[]{:S(2)}) async-start(bf16[16,16,2048]{2,1,0:T(8,128)(2,1)} %bitcast.2), calls=%async_computation | async-start | bytes 2097152 | tf_op jit(solution)/shard_map/all_to_all | solution.py:352
  28.3 159.2 %all-gather.7.cloned.1.call-start = ((), (), s32[]{:S(2)}) async-start(), calls=%async_computation.4 | async-start | bytes 4456448 | tf_op jit(solution)/shard_map/all_gather | solution.py:371
  28.6 10.2 %collective-permute-start.17 = (bf16[128,128]{1,0:T(8,128)(2,1)S(1)}, bf16[128,128]{1,0:T(8,128)(2,1)S(1)}, u32[]{:S(2)}, u32[]{:S(2)}) collective-permute-start(bf16[128,128]{1,0:T(8,128)(2,1)S(1)} %pad_maximum_fusion.2.refs_0_), channel_id=1, source_target_pairs={{0,14},{1,15},{2,0},{3,1},{4,2},{5,3},{6,4},{7,5},{8,6},{9,7},{10,... | collective-permute-start | bytes 98312 | tf_op jit(solution)/shard_map/ppermute | solution.py:362
  32.3 9.6 %collective-permute-start.18 = (bf16[128,128]{1,0:T(8,128)(2,1)S(1)}, bf16[128,128]{1,0:T(8,128)(2,1)S(1)}, u32[]{:S(2)}, u32[]{:S(2)}) collective-permute-start(bf16[128,128]{1,0:T(8,128)(2,1)S(1)} %pad_maximum_fusion.2.refs_0_), channel_id=1, source_target_pairs={{0,12},{1,13},{2,14},{3,15},{4,0},{5,1},{6,2},{7,3},{8,4},{9,5},{1... | collective-permute-start | bytes 98312 | tf_op jit(solution)/shard_map/ppermute | solution.py:362
  33.3 10.5 %collective-permute-start.19 = (bf16[128,128]{1,0:T(8,128)(2,1)S(1)}, bf16[128,128]{1,0:T(8,128)(2,1)S(1)}, u32[]{:S(2)}, u32[]{:S(2)}) collective-permute-start(bf16[128,128]{1,0:T(8,128)(2,1)S(1)} %pad_maximum_fusion.2.refs_0_), channel_id=1, source_target_pairs={{0,10},{1,11},{2,12},{3,13},{4,14},{5,15},{6,0},{7,1},{8,2},{9,3},... | collective-permute-start | bytes 98312 | tf_op jit(solution)/shard_map/ppermute | solution.py:362
  34.3 9.4 %collective-permute-start.20 = (bf16[128,128]{1,0:T(8,128)(2,1)S(1)}, bf16[128,128]{1,0:T(8,128)(2,1)S(1)}, u32[]{:S(2)}, u32[]{:S(2)}) collective-permute-start(bf16[128,128]{1,0:T(8,128)(2,1)S(1)} %pad_maximum_fusion.2.refs_0_), channel_id=1, source_target_pairs={{0,8},{1,9},{2,10},{3,11},{4,12},{5,13},{6,14},{7,15},{8,0},{9,1},... | collective-permute-start | bytes 98312 | tf_op jit(solution)/shard_map/ppermute | solution.py:362
  38.8 7.1 %collective-permute-start.21 = (bf16[128,128]{1,0:T(8,128)(2,1)S(1)}, bf16[128,128]{1,0:T(8,128)(2,1)S(1)}, u32[]{:S(2)}, u32[]{:S(2)}) collective-permute-start(bf16[128,128]{1,0:T(8,128)(2,1)S(1)} %pad_maximum_fusion.2.refs_0_), channel_id=1, source_target_pairs={{0,6},{1,7},{2,8},{3,9},{4,10},{5,11},{6,12},{7,13},{8,14},{9,15},... | collective-permute-start | bytes 98312 | tf_op jit(solution)/shard_map/ppermute | solution.py:362
  38.8 8.1 %collective-permute-start.22 = (bf16[128,128]{1,0:T(8,128)(2,1)S(1)}, bf16[128,128]{1,0:T(8,128)(2,1)S(1)}, u32[]{:S(2)}, u32[]{:S(2)}) collective-permute-start(bf16[128,128]{1,0:T(8,128)(2,1)S(1)} %pad_maximum_fusion.2.refs_0_), channel_id=1, source_target_pairs={{0,4},{1,5},{2,6},{3,7},{4,8},{5,9},{6,10},{7,11},{8,12},{9,13},{1... | collective-permute-start | bytes 98312 | tf_op jit(solution)/shard_map/ppermute | solution.py:362
  41.9 5.3 %collective-permute-start.23 = (bf16[128,128]{1,0:T(8,128)(2,1)S(1)}, bf16[128,128]{1,0:T(8,128)(2,1)S(1)}, u32[]{:S(2)}, u32[]{:S(2)}) collective-permute-start(bf16[128,128]{1,0:T(8,128)(2,1)S(1)} %pad_maximum_fusion.2.refs_0_), channel_id=1, source_target_pairs={{0,2},{1,3},{2,4},{3,5},{4,6},{5,7},{6,8},{7,9},{8,10},{9,11},{10,... | collective-permute-start | bytes 98312 | tf_op jit(solution)/shard_map/ppermute | solution.py:362
  49.2 27.4 %collective-permute-start = (bf16[2,2048,128]{2,1,0:T(8,128)(2,1)S(1)}, bf16[2,2048,128]{2,1,0:T(8,128)(2,1)}, u32[]{:S(2)}, u32[]{:S(2)}) collective-permute-start(bf16[2,2048,128]{2,1,0:T(8,128)(2,1)S(1)} %constant_dynamic-update-slice_fusion.refs_1_), channel_id=1, source_target_pairs={{0,2},{1,15},{2,4},{3,1},{4,6},{5,3},{6,8},{7,5},{8,10},{9,7},{10,... | collective-permute-start | bytes 3145736 | tf_op jit(solution)/shard_map/ppermute | solution.py:334
  50.0 26.6 %collective-permute-start.1 = (bf16[2,2048,128]{2,1,0:T(8,128)(2,1)S(1)}, bf16[2,2048,128]{2,1,0:T(8,128)(2,1)}, u32[]{:S(2)}, u32[]{:S(2)}) collective-permute-start(bf16[2,2048,128]{2,1,0:T(8,128)(2,1)S(1)} %constant_dynamic-update-slice_fusion.refs_1_), channel_id=1, source_target_pairs={{0,14},{1,3},{2,0},{3,5},{4,2},{5,7},{6,4},{7,9},{8,6},{9,11},{10,... | collective-permute-start | bytes 3145736 | tf_op jit(solution)/shard_map/ppermute | solution.py:334
  52.5 28.1 %copy-start.23 = (bf16[16,16,2048]{2,1,0:T(8,128)(2,1)}, bf16[16,16,2048]{2,1,0:T(8,128)(2,1)S(1)}, u32[]{:S(2)}) copy-start(bf16[16,16,2048]{2,1,0:T(8,128)(2,1)S(1)} %all-to-all-done) | copy-start | bytes 3145732
  52.5 28.1 %collective-permute-start.4 = (bf16[256,2048]{1,0:T(8,128)(2,1)S(1)}, bf16[256,2048]{1,0:T(8,128)(2,1)}, u32[]{:S(2)}, u32[]{:S(2)}) collective-permute-start(bf16[256,2048]{1,0:T(8,128)(2,1)S(1)} %bitcast.24), channel_id=1, source_target_pairs={{0,1},{1,0},{2,3},{3,2},{4,5},{5,4},{6,7},{7,6},{8,9},{9,8},{10,11... | collective-permute-start | bytes 3145736 | tf_op jit(solution)/shard_map/ppermute | solution.py:373
  52.7 35.0 %collective-permute-start.8 = (bf16[128,2048]{1,0:T(8,128)(2,1)}, bf16[128,2048]{1,0:T(8,128)(2,1)S(1)}, u32[]{:S(2)}, u32[]{:S(2)}) collective-permute-start(bf16[128,2048]{1,0:T(8,128)(2,1)} %collective-permute-done.5.refs_4_), channel_id=1, source_target_pairs={{0,2},{1,15},{2,4},{3,1},{4,6},{5,3},{6,8},{7,5},{8,10},{9,7},{10,... | collective-permute-start | bytes 1572872 | tf_op jit(solution)/shard_map/ppermute | solution.py:334
  52.8 35.8 %collective-permute-start.9 = (bf16[128,2048]{1,0:T(8,128)(2,1)}, bf16[128,2048]{1,0:T(8,128)(2,1)S(1)}, u32[]{:S(2)}, u32[]{:S(2)}) collective-permute-start(bf16[128,2048]{1,0:T(8,128)(2,1)} %collective-permute-done.6.refs_2_), channel_id=1, source_target_pairs={{0,14},{1,3},{2,0},{3,5},{4,2},{5,7},{6,4},{7,9},{8,6},{9,11},{10,... | collective-permute-start | bytes 1572872 | tf_op jit(solution)/shard_map/ppermute | solution.py:334
  77.1 5.1 %copy-start.8 = (bf16[1,128,2048]{2,1,0:T(8,128)(2,1)S(1)}, bf16[1,128,2048]{2,1,0:T(8,128)(2,1)}, u32[]{:S(2)}) copy-start(bf16[1,128,2048]{2,1,0:T(8,128)(2,1)} %param.21) | copy-start | bytes 1572868
  77.2 30.2 %collective-permute-start.2 = (bf16[2,2048,128]{2,1,0:T(8,128)(2,1)}, bf16[2,2048,128]{2,1,0:T(8,128)(2,1)}, u32[]{:S(2)}, u32[]{:S(2)}) collective-permute-start(bf16[2,2048,128]{2,1,0:T(8,128)(2,1)} %collective-permute-done.refs_2_), channel_id=1, source_target_pairs={{0,2},{1,15},{2,4},{3,1},{4,6},{5,3},{6,8},{7,5},{8,10},{9,7},{10,... | collective-permute-start | bytes 3145736 | tf_op jit(solution)/shard_map/ppermute | solution.py:334
  77.2 30.1 %collective-permute-start.3 = (bf16[2,2048,128]{2,1,0:T(8,128)(2,1)}, bf16[2,2048,128]{2,1,0:T(8,128)(2,1)}, u32[]{:S(2)}, u32[]{:S(2)}) collective-permute-start(bf16[2,2048,128]{2,1,0:T(8,128)(2,1)} %collective-permute-done.1.refs_1_), channel_id=1, source_target_pairs={{0,14},{1,3},{2,0},{3,5},{4,2},{5,7},{6,4},{7,9},{8,6},{9,11},{10,... | collective-permute-start | bytes 3145736 | tf_op jit(solution)/shard_map/ppermute | solution.py:334
  90.9 5.0 %copy-start.18 = (bf16[1024,128]{1,0:T(8,128)(2,1)S(1)}, bf16[1024,128]{1,0:T(8,128)(2,1)}, u32[]{:S(2)}) copy-start(bf16[1024,128]{1,0:T(8,128)(2,1)} %concatenate.23.q_ref) | copy-start | bytes 786436
  95.9 2.3 %copy-start.21 = (bf16[16896,128]{1,0:T(8,128)(2,1)S(1)}, bf16[16896,128]{1,0:T(8,128)(2,1)}, u32[]{:S(2)}) copy-start(bf16[16896,128]{1,0:T(8,128)(2,1)} %all-gather.5.cloned.1.call-done) | copy-start | bytes 12976132
  98.2 12.4 %copy-start.10 = (bf16[128,2048]{1,0:T(8,128)(2,1)S(1)}, bf16[128,2048]{1,0:T(8,128)(2,1)}, u32[]{:S(2)}) copy-start(bf16[128,2048]{1,0:T(8,128)(2,1)} %copy-done.9) | copy-start | bytes 1572868
  98.2 12.4 %copy-start.12 = (bf16[128,2048]{1,0:T(8,128)(2,1)S(1)}, bf16[128,2048]{1,0:T(8,128)(2,1)}, u32[]{:S(2)}) copy-start(bf16[128,2048]{1,0:T(8,128)(2,1)} %copy-done.11) | copy-start | bytes 1572868
  98.2 15.7 %copy-start.22 = (bf16[16896,128]{1,0:T(8,128)(2,1)S(1)}, bf16[16896,128]{1,0:T(8,128)(2,1)}, u32[]{:S(2)}) copy-start(bf16[16896,128]{1,0:T(8,128)(2,1)} %all-gather.5.cloned.1.call-done) | copy-start | bytes 12976132
  107.4 36.2 %copy-start.3 = (bf16[512,2048]{1,0:T(8,128)(2,1)S(1)}, bf16[512,2048]{1,0:T(8,128)(2,1)}, u32[]{:S(2)}) copy-start(bf16[512,2048]{1,0:T(8,128)(2,1)} %experts.7.refs_5_) | copy-start | bytes 6291460
  107.4 41.2 %collective-permute-start.10 = (bf16[2,2048,128]{2,1,0:T(8,128)(2,1)}, bf16[2,2048,128]{2,1,0:T(8,128)(2,1)}, u32[]{:S(2)}, u32[]{:S(2)}) collective-permute-start(bf16[2,2048,128]{2,1,0:T(8,128)(2,1)} %collective-permute-done.2.refs_1_), channel_id=1, source_target_pairs={{0,2},{1,15},{2,4},{3,1},{4,6},{5,3},{6,8},{7,5},{8,10},{9,7},{10,... | collective-permute-start | bytes 3145736 | tf_op jit(solution)/shard_map/ppermute | solution.py:334
  107.6 41.0 %collective-permute-start.11 = (bf16[2,2048,128]{2,1,0:T(8,128)(2,1)}, bf16[2,2048,128]{2,1,0:T(8,128)(2,1)S(1)}, u32[]{:S(2)}, u32[]{:S(2)}) collective-permute-start(bf16[2,2048,128]{2,1,0:T(8,128)(2,1)} %collective-permute-done.3.refs_2_), channel_id=1, source_target_pairs={{0,14},{1,3},{2,0},{3,5},{4,2},{5,7},{6,4},{7,9},{8,6},{9,11},{10,... | collective-permute-start | bytes 3145736 | tf_op jit(solution)/shard_map/ppermute | solution.py:334
  110.6 33.0 %collective-permute-start.12 = (bf16[128,2048]{1,0:T(8,128)(2,1)S(1)}, bf16[128,2048]{1,0:T(8,128)(2,1)S(1)}, u32[]{:S(2)}, u32[]{:S(2)}) collective-permute-start(bf16[128,2048]{1,0:T(8,128)(2,1)S(1)} %copy-done.10), channel_id=1, source_target_pairs={{0,2},{1,15},{2,4},{3,1},{4,6},{5,3},{6,8},{7,5},{8,10},{9,7},{10,... | collective-permute-start | bytes 1572872 | tf_op jit(solution)/shard_map/ppermute | solution.py:334
  110.6 33.0 %collective-permute-start.13 = (bf16[128,2048]{1,0:T(8,128)(2,1)S(1)}, bf16[128,2048]{1,0:T(8,128)(2,1)}, u32[]{:S(2)}, u32[]{:S(2)}) collective-permute-start(bf16[128,2048]{1,0:T(8,128)(2,1)S(1)} %copy-done.12), channel_id=1, source_target_pairs={{0,14},{1,3},{2,0},{3,5},{4,2},{5,7},{6,4},{7,9},{8,6},{9,11},{10,... | collective-permute-start | bytes 1572872 | tf_op jit(solution)/shard_map/ppermute | solution.py:334
  114.7 38.1 %copy-start.19 = (bf16[512,128]{1,0:T(8,128)(2,1)}, bf16[512,128]{1,0:T(8,128)(2,1)S(1)}, u32[]{:S(2)}) copy-start(bf16[512,128]{1,0:T(8,128)(2,1)S(1)} %attend.3) | copy-start | bytes 393220
  143.6 4.9 %copy-start.13 = (bf16[128,2048]{1,0:T(8,128)(2,1)}, bf16[128,2048]{1,0:T(8,128)(2,1)S(1)}, u32[]{:S(2)}) copy-start(bf16[128,2048]{1,0:T(8,128)(2,1)S(1)} %collective-permute-done.12.refs_3_) | copy-start | bytes 1572868
  149.6 23.3 %collective-permute-start.14 = (bf16[2,2048,128]{2,1,0:T(8,128)(2,1)}, bf16[2,2048,128]{2,1,0:T(8,128)(2,1)S(1)}, u32[]{:S(2)}, u32[]{:S(2)}) collective-permute-start(bf16[2,2048,128]{2,1,0:T(8,128)(2,1)} %collective-permute-done.10.refs_1_), channel_id=1, source_target_pairs={{0,2},{1,15},{2,4},{3,1},{4,6},{5,3},{6,8},{7,5},{8,10},{9,7},{10,... | collective-permute-start | bytes 3145736 | tf_op jit(solution)/shard_map/ppermute | solution.py:395
  149.6 16.9 %collective-permute-start.15 = (bf16[128,2048]{1,0:T(8,128)(2,1)}, bf16[128,2048]{1,0:T(8,128)(2,1)}, u32[]{:S(2)}, u32[]{:S(2)}) collective-permute-start(bf16[128,2048]{1,0:T(8,128)(2,1)} %collective-permute-done.13.refs_4_), channel_id=1, source_target_pairs={{0,14},{1,3},{2,0},{3,5},{4,2},{5,7},{6,4},{7,9},{8,6},{9,11},{10,... | collective-permute-start | bytes 1572872 | tf_op jit(solution)/shard_map/ppermute | solution.py:388
  152.8 20.1 %all-to-all-start.1 = ((bf16[16,32,128]{2,1,0:T(8,128)(2,1)}), bf16[16,32,128]{2,1,0:T(8,128)(2,1)S(1)}, u32[]{:S(2)}, u32[]{:S(2)}) async-start(bf16[16,32,128]{2,1,0:T(8,128)(2,1)} %bitcast.20), calls=%async_computation.1 | async-start | bytes 262144 | tf_op jit(solution)/shard_map/all_to_all | solution.py:391
  172.9 1.6 copy-start.1
  176.8 2.7 %collective-permute-start.16 = (bf16[256,2048]{1,0:T(8,128)(2,1)S(1)}, bf16[256,2048]{1,0:T(8,128)(2,1)S(1)}, u32[]{:S(2)}, u32[]{:S(2)}) collective-permute-start(bf16[256,2048]{1,0:T(8,128)(2,1)S(1)} %experts.11), channel_id=1, source_target_pairs={{0,1},{1,0},{2,3},{3,2},{4,5},{5,4},{6,7},{7,6},{8,9},{9,8},{10,11... | collective-permute-start | bytes 3145736 | tf_op jit(solution)/shard_map/ppermute | solution.py:400
  179.3 8.1 %copy-start.26 = (f32[96,2]{0,1:T(2,128)S(1)}, f32[96,2]{0,1:T(2,128)}, u32[]{:S(2)}) copy-start(f32[96,2]{0,1:T(2,128)} %param.23) | copy-start | bytes 2308
  181.0 22.6 %all-to-all-start.2 = ((bf16[16,16,2048]{2,1,0:T(8,128)(2,1)}), bf16[16,16,2048]{2,1,0:T(8,128)(2,1)S(1)}, u32[]{:S(2)}, u32[]{:S(2)}) async-start(bf16[16,16,2048]{2,1,0:T(8,128)(2,1)} %bitcast.9), calls=%async_computation.2 | async-start | bytes 2097152 | tf_op jit(solution)/shard_map/all_to_all | solution.py:403
  187.5 2.2 %copy-start.5 = (bf16[16384,128]{1,0:T(8,128)(2,1)S(1)}, bf16[16384,128]{1,0:T(8,128)(2,1)}, u32[]{:S(2)}) copy-start(bf16[16384,128]{1,0:T(8,128)(2,1)} %all-gather.7.cloned.1.call-done) | copy-start | bytes 12582916
  189.7 13.8 %copy-start.16 = (s32[96,2]{1,0:T(8,128)S(1)}, s32[96,2]{1,0:T(8,128)}, u32[]{:S(2)}) copy-start(s32[96,2]{1,0:T(8,128)} %copy-done.15) | copy-start | bytes 2308
  (8 other events, 8.8 us)
Sparse Core Ops, SparseCore 0:
  11.3 69.4 all-gather.4
  83.2 56.2 all-gather.6
where the time goes:
time: 214 us; the launch traced here: 212 us
  waiting for transfers between devices  75.3 us (35%)
  starting transfers between devices  59.6 us (28%)
  Pallas kernels  36.2 us (17%)
  local copies, waits for them, and re-layouts  21.8 us (10%)
  between operations  14.3 us (7%)
  other arithmetic  4.82 us (2%)
    ppermute x12, waiting for transfers between devices, ring(): return (lax.ppermute(a, 'tp', ahead), lax.ppermute(b, 'tp', back))  54.1 us
    pallas_call x6, Pallas kernels, experts(): pl.pallas_call(body, grid=(count,), in_specs=specs, out_specs=pl.BlockSpe...  23.7 us
    ppermute x12, starting transfers between devices, ring(): return (lax.ppermute(a, 'tp', ahead), lax.ppermute(b, 'tp', back))  22.5 us
    unnamed x60, local copies, waits for them, and re-layouts  18.1 us
    ppermute x7, starting transfers between devices, local(): lax.ppermute(strip, 'tp', [(2 * z + c, 2 * ((z - s) % chips) + c) for z,...  15.1 us
    all_to_all x1, waiting for transfers between devices, local(): lax.all_to_all(results, 'ep', split_axis=0, concat_axis=0, tiled=True)  10.2 us
    all_to_all x1, starting transfers between devices, local(): lax.all_to_all(outgoing, 'ep', split_axis=0, concat_axis=0, tiled=True)  7.61 us
    all_to_all x1, waiting for transfers between devices, local(): lax.all_to_all(attention.reshape(n_tp, -1, 2 * HEAD), 'tp', split_axis=0,...  6.48 us
  transfers between devices with their start and end apart: 29, of which 13 were waited for; matrix products, arithmetic and copies ran while one was open for 4% of the time, Pallas kernels for 16%

commit v1 on v0

--- a/solution.py
+++ b/solution.py
@@ -20,6 +20,10 @@
 
 def whole(shape):
     return pl.BlockSpec(shape, lambda *_: (0,) * len(shape))
+
+
+def held(*arrays):
+    return [pltpu.with_memory_space_constraint(a, pltpu.HBM) for a in arrays]
 
 
 def params(limit=16 << 20):
@@ -98,58 +102,155 @@
     return lax.dot_general(a, b, (((1,), (1,)), ((), ())), preferred_element_type=F32)
 
 
-def hidden(rows, gu_refs):
-    acts = []
-    for gu in gu_refs:
-        pre = jnp.dot(
-            rows, jnp.concatenate([gu[0], gu[1]], axis=1), preferred_element_type=F32
-        )
-        acts.append(gated(pre[:, :128], pre[:, 128:]))
-    return jnp.concatenate(acts, axis=1) if len(acts) > 1 else acts[0]
-
-
-def stacked(d_refs):
-    downs = [d[...] for d in d_refs]
-    return jnp.concatenate(downs, axis=0) if len(downs) > 1 else downs[0]
-
-
-def experts(x, gus, downs, y, first=0, count=None, keep=True):
-    d = x.shape[1]
-    n = len(gus)
-    count = x.shape[0] // 256 if count is None else count
+def experts(rows, gus, downs, y, first=0):
+    n, m = len(gus), len(rows)
+    count, d = sum(r.shape[0] for r in rows), rows[0].shape[1]
+    each, wide = count // m, 512
+    has_y = y is not None
 
     def body(*refs):
-        x_ref, gu_refs, d_refs, out_ref = refs[0], refs[1 : 1 + n], refs[1 + n : 1 + 2 * n], refs[-1]
-        total = jnp.dot(
-            hidden(x_ref[...], gu_refs), stacked(d_refs), preferred_element_type=F32
-        )
-        if y is not None:
-            total = total + refs[-2][...].astype(F32)
-        out_ref[...] = total.astype(BF16)
-
-    rows = pl.BlockSpec((256, d), lambda i: (i + first, 0))
-    args = [x, *gus, *downs] + ([] if y is None else [y])
-    specs = [rows] + [whole(w.shape) for w in (*gus, *downs)] + ([] if y is None else [rows])
+        row_refs, refs = refs[:m], refs[m:]
+        gu_refs, refs = refs[:n], refs[n:]
+        d_refs, refs = refs[:n], refs[n:]
+        if has_y:
+            y_ref, refs = refs[0], refs[1:]
+        out_ref, x, gu, down, acts, old, new, sems, out_sems = refs
+        x_in = [
+            pltpu.make_async_copy(row_refs[k], x.at[pl.ds(k * each, each), :], sems.at[k])
+            for k in range(m)
+        ]
+        gu_in = [pltpu.make_async_copy(gu_refs[c], gu.at[c], sems.at[m + c]) for c in range(n)]
+        d_in = [
+            pltpu.make_async_copy(
+                d_refs[c], down.at[pl.ds(c * 128, 128), :], sems.at[m + n + c]
+            )
+            for c in range(n)
+        ]
+        for copy in x_in + gu_in + d_in:
+            copy.start()
+        if has_y:
+            y_in = pltpu.make_async_copy(
+                y_ref.at[pl.ds(first, count), :], old, sems.at[m + 2 * n]
+            )
+            y_in.start()
+        for copy in x_in:
+            copy.wait()
+
+        def slice_of_hidden(c, carry):
+            pltpu.make_async_copy(gu_refs[0], gu.at[c], sems.at[m + c]).wait()
+            pre = jnp.dot(
+                x[...], jnp.concatenate([gu[c, 0], gu[c, 1]], axis=1), preferred_element_type=F32
+            )
+            at = pl.multiple_of(c * 128, 128)
+            acts[:, pl.ds(at, 128)] = gated(pre[:, :128], pre[:, 128:])
+            return carry
+
+        lax.fori_loop(0, n, slice_of_hidden, 0)
+        for copy in d_in:
+            copy.wait()
+        if has_y:
+            y_in.wait()
+
+        def out_copy(t):
+            to = pl.ds(pl.multiple_of(t * wide, wide), wide)
+            return pltpu.make_async_copy(new.at[:, to], out_ref.at[:, to], out_sems.at[t])
+
+        def slice_of_out(t, carry):
+            at = pl.ds(pl.multiple_of(t * wide, wide), wide)
+            total = jnp.dot(acts[...], down[:, at], preferred_element_type=F32)
+            if has_y:
+                total = total + old[:, at].astype(F32)
+            new[:, at] = total.astype(BF16)
+            out_copy(t).start()
+            return carry
+
+        lax.fori_loop(0, d // wide, slice_of_out, 0)
+        for t in range(d // wide):
+            out_copy(t).wait()
+
+    args = held(*rows, *gus, *downs, *([y] if has_y else []))
+    hbm = pl.BlockSpec(memory_space=pltpu.HBM)
     return pl.pallas_call(
         body,
-        grid=(count,),
-        in_specs=specs,
-        out_specs=pl.BlockSpec((256, d), lambda i: (i, 0)),
-        out_shape=pltpu.HBM((count * 256, d), BF16) if keep else jax.ShapeDtypeStruct((count * 256, d), BF16),
-        compiler_params=params(),
+        in_specs=[hbm] * len(args),
+        out_specs=hbm,
+        out_shape=pltpu.HBM((count, d), BF16),
+        scratch_shapes=[
+            pltpu.VMEM((count, d), BF16),
+            pltpu.VMEM((n, 2, d, 128), BF16),
+            pltpu.VMEM((n * 128, d), BF16),
+            pltpu.VMEM((count, n * 128), BF16),
+            pltpu.VMEM((count, d) if has_y else (16, 128), BF16),
+            pltpu.VMEM((count, d), BF16),
+            pltpu.SemaphoreType.DMA((m + 2 * n + 1,)),
+            pltpu.SemaphoreType.DMA((d // wide,)),
+        ],
+        compiler_params=params(24 << 20),
         name="experts",
         cost_estimate=pl.CostEstimate(
-            flops=6 * count * 256 * d * 128 * n,
-            transcendentals=count * 256 * 128,
+            flops=6 * count * d * 128 * n,
+            transcendentals=count * 128 * n,
             bytes_accessed=6 << 20,
         ),
     )(*args)
 
 
+def experts_last(rows, gu, down, y, first):
+    count, d = rows.shape
+
+    def body(x_ref, gu_ref, d_ref, y_ref, out_ref):
+        both = jnp.concatenate([gu_ref[0], gu_ref[1]], axis=1)
+        pre = jnp.dot(x_ref[...], both, preferred_element_type=F32)
+        total = jnp.dot(
+            gated(pre[:, :128], pre[:, 128:]), d_ref[...], preferred_element_type=F32
+        )
+        out_ref[...] = (total + y_ref[...].astype(F32)).astype(BF16)
+
+    x, old = held(rows, y)
+    return pl.pallas_call(
+        body,
+        grid=(1,),
+        in_specs=[
+            whole((count, d)),
+            whole(gu.shape),
+            whole(down.shape),
+            pl.BlockSpec((count, d), lambda i: (first // count, 0)),
+        ],
+        out_specs=whole((count, d)),
+        out_shape=jax.ShapeDtypeStruct((count, d), BF16),
+        compiler_params=params(),
+        name="experts_last",
+        cost_estimate=pl.CostEstimate(
+            flops=6 * count * d * 128, transcendentals=count * 128, bytes_accessed=5 << 20
+        ),
+    )(x, gu, down, old)
+
+
+def widen(queries):
+    def body(q_ref, out_ref):
+        scaled = (q_ref[...].astype(F32) * 0.125).astype(BF16)
+        out_ref[...] = jnp.concatenate([scaled, jnp.zeros_like(scaled)], axis=1)
+
+    return pl.pallas_call(
+        body,
+        out_shape=jax.ShapeDtypeStruct((queries.shape[0], 2 * queries.shape[1]), BF16),
+        compiler_params=params(),
+        name="widen",
+    )(queries)
+
+
 def attend(ep, base, q, kvg, state, first, last, finish):
     tiles = BLOCK // TILE
 
-    def body(ep_ref, base_ref, q_ref, kv_ref, *rest):
+    def body(ep_ref, base_ref, q_ref, kvg_ref, *rest):
+        kv_ref, sems = rest[-2:]
+        rest = rest[:-2]
+
+        def fetch(j):
+            return pltpu.make_async_copy(kvg_ref.at[first + j], kv_ref.at[j], sems.at[j])
+
+        for j in range(last - first):
+            fetch(j).start()
         if state is not None:
             m_in, acc_in = rest[0], rest[1]
             rest = rest[2:]
@@ -168,6 +269,7 @@
         lane = lax.broadcasted_iota(jnp.int32, (BLOCK, 128), 1)
 
         def one(j, masked):
+            fetch(j).wait()
             kv = kv_ref[j, 0:BLOCK, :]
             parts = kv_ref[j, BLOCK : BLOCK + 32, :].astype(F32)
             gates = (parts[0:8] + parts[8:16]) + parts[16:24]
@@ -178,11 +280,7 @@
             def scores(t):
                 return nt(q_ref[t * TILE : (t + 1) * TILE, :], kv)
 
-            ahead = scores(0)
-            for t in range(tiles):
-                s = ahead
-                if t + 1 < tiles:
-                    ahead = scores(t + 1)
+            def update(t, s):
                 at = slice(t * TILE, (t + 1) * TILE)
                 s = s + row
                 if masked:
@@ -199,6 +297,13 @@
                 )
                 m_ref[at, :] = peak
 
+            ahead = scores(0)
+            for t in range(tiles):
+                s = ahead
+                if t + 1 < tiles:
+                    ahead = scores(t + 1)
+                update(t, s)
+
         def step(j, carry):
             one(j - first, False)
             return carry
@@ -208,6 +313,12 @@
         @pl.when((me >= first) & (me < last))
         def _():
             one(me - first, True)
+
+        def drop(j, carry):
+            fetch(j - first).wait()
+            return carry
+
+        lax.fori_loop(jnp.maximum(jnp.minimum(me + 1, last), first), last, drop, 0)
 
         if finish:
             for g in range(BLOCK // 64):
@@ -217,12 +328,12 @@
                 out_ref[32 * g : 32 * g + 32, :] = jnp.concatenate(pair, axis=1).astype(BF16)
 
     span = last - first
-    args = [ep, base, q, kvg]
+    args = [ep, base, q, *held(kvg)]
     specs = [
         pl.BlockSpec(memory_space=pltpu.SMEM),
         whole(base.shape),
         whole(q.shape),
-        pl.BlockSpec((span,) + kvg.shape[1:], lambda *_: (first // span, 0, 0)),
+        pl.BlockSpec(memory_space=pltpu.HBM),
     ]
     wide = jax.ShapeDtypeStruct((BLOCK, 128), F32)
     if state is not None:
@@ -242,7 +353,8 @@
         in_specs=specs,
         out_specs=out_specs,
         out_shape=outs,
-        scratch_shapes=scratch,
+        scratch_shapes=scratch
+        + [pltpu.VMEM((span,) + kvg.shape[1:], BF16), pltpu.SemaphoreType.DMA((span,))],
         compiler_params=params(),
         name="attend",
         cost_estimate=pl.CostEstimate(
@@ -251,29 +363,31 @@
     )(*args)
 
 
-def arrange(place, near):
-    n = len(near)
-
-    def body(place_ref, *refs):
-        out_ref = refs[-1]
+def arrange(place, low, high, far):
+    each = low.shape[0] // HEAD
+
+    def body(place_ref, low_ref, high_ref, far_ref, out_ref):
         chip = lax.div(place_ref[0], 2)
         core = lax.rem(place_ref[0], 2)
-        for s in range(n):
-            at = lax.rem(chip + s, n) * 2 * HEAD
+        for k in range(2 * each):
+            at = jnp.bitwise_xor(chip, k) * 2 * HEAD
             mine = pl.multiple_of(at + core * HEAD, HEAD)
             other = pl.multiple_of(at + (1 - core) * HEAD, HEAD)
-            out_ref[pl.ds(mine, HEAD), :] = refs[s][:HEAD, :]
-            out_ref[pl.ds(other, HEAD), :] = refs[s][HEAD:, :]
+            near = low_ref if k < each else high_ref
+            piece = slice((k % each) * HEAD, (k % each + 1) * HEAD)
+            out_ref[pl.ds(mine, HEAD), :] = near[piece, :]
+            out_ref[pl.ds(other, HEAD), :] = far_ref[k * HEAD : (k + 1) * HEAD, :]
 
     return pl.pallas_call(
         body,
         grid=(1,),
-        in_specs=[pl.BlockSpec(memory_space=pltpu.SMEM)] + [whole(a.shape) for a in near],
-        out_specs=whole((n * 2 * HEAD, 128)),
-        out_shape=jax.ShapeDtypeStruct((n * 2 * HEAD, 128), BF16),
+        in_specs=[pl.BlockSpec(memory_space=pltpu.SMEM)]
+        + [whole(a.shape) for a in (low, high, far)],
+        out_specs=whole((2 * far.shape[0], 128)),
+        out_shape=jax.ShapeDtypeStruct((2 * far.shape[0], 128), BF16),
         compiler_params=params(),
         name="arrange",
-    )(place, *near)
+    )(place, low, high, far)
 
 
 def project(packed, columns):
@@ -333,11 +447,13 @@
     def ring(a, b):
         return lax.ppermute(a, "tp", ahead), lax.ppermute(b, "tp", back)
 
+    def across(a, bit):
+        return lax.ppermute(a, "tp", [(2 * z + c, 2 * (z ^ bit) + c) for z, c in spot])
+
+    strip = lax.dynamic_slice_in_dim(out_weight, lax.axis_index("ep") * 128, 128, 1)
+    strip = jnp.concatenate([strip, across(strip, 1)], axis=0)
     down = down_weight[0]
     da1, db1 = ring(down, down)
-    gu = jnp.concatenate([gate_weight, up_weight], axis=0)
-    ga1, gb1 = ring(gu, gu)
-
     high = lax.reduce_precision(cumulative_gate, 8, 7)
     mid = lax.reduce_precision(cumulative_gate - high, 8, 7)
     low = cumulative_gate - high - mid
@@ -346,59 +462,55 @@
     packed = jnp.concatenate(
         [jnp.concatenate([key_vectors, value_vectors], axis=1), gates], axis=0
     )
+    kvg = lax.all_gather(packed, "ep", axis=0)
+    packed, gate_weight, strip = fence((packed, gate_weight, strip))
+    strip = jnp.concatenate([strip, across(strip, 2)], axis=0)
+    gu = jnp.concatenate([gate_weight, up_weight], axis=0)
+    ga1, gb1 = ring(gu, gu)
+
     gain = norm_gain[None, :]
     outgoing = dispatch(expert_tokens, gain, expert_choice).reshape(n_ep, PAD, d)
-    kvg = lax.all_gather(packed, "ep", axis=0)
     arrived = lax.all_to_all(outgoing, "ep", split_axis=0, concat_axis=0, tiled=True)
     ep = lax.axis_index("ep").astype(jnp.int32).reshape(1)
-    q = jnp.concatenate([queries * BF16(0.125), jnp.zeros_like(queries)], axis=1)
+    strips_high = across(strip, 4)
+    q = widen(queries)
     base = jnp.broadcast_to(cumulative_gate[0:1, :], (1, 128))
-    strip = lax.dynamic_slice_in_dim(out_weight, lax.axis_index("ep") * 128, 128, 1)
-    strip = jnp.concatenate([strip, lax.ppermute(strip, "tp", swap)], axis=0)
-    da1, db1, strip = fence((da1, db1, strip))
+    da1, db1 = fence((da1, db1))
 
     da2, db2 = ring(da1, db1)
-    near = [strip] + [
-        lax.ppermute(
-            strip, "tp", [(2 * z + c, 2 * ((z - s) % chips) + c) for z, c in spot]
-        )
-        for s in range(1, chips)
-    ]
-    strips = arrange(lax.axis_index("tp").astype(jnp.int32).reshape(1), near)
     ga1, gb1, q, base = fence((ga1, gb1, q, base))
 
     ga2, gb2 = ring(ga1, gb1)
+    far = lax.ppermute(jnp.concatenate([strip, strips_high], axis=0), "tp", swap)
+    place = lax.axis_index("tp").astype(jnp.int32).reshape(1)
+    strips = arrange(place, strip, strips_high, far)
     columns = lax.all_gather(strips, "ep", axis=0)
     arrived = arrived.reshape(n_ep * PAD, d)
     beside = lax.ppermute(arrived, "tp", swap)
-    x = jnp.concatenate([arrived, beside], axis=0)
-    y = experts(x, [gu, ga1], [down, da1], None)
-    da2, db2, y = fence((da2, db2, y))
+    x = [arrived, beside]
+    da2, db2 = fence((da2, db2))
 
     da3, db3 = ring(da2, db2)
     half = n_ep // 2
-    y = experts(x, [gb1], [db1], y)
+    y = experts(x, [gu, ga1, gb1], [down, da1, db1], None)
     state = attend(ep, base, q, kvg, None, 0, half, False)
-    ga2, gb2, y, state = fence((ga2, gb2, y, state))
+    ga2, gb2, state = fence((ga2, gb2, state))
 
     ga3, gb3 = ring(ga2, gb2)
+    d4 = lax.ppermute(db3, "tp", back)
     attention = attend(ep, base, q, kvg, state, half, n_ep, True)
-    da3, db3, attention = fence((da3, db3, attention))
-
-    d4 = lax.ppermute(db3, "tp", back)
-    y = experts(x, [ga2, gb2], [da2, db2], y)
-    ga3, gb3, y, attention = fence((ga3, gb3, y, attention))
     rows = lax.all_to_all(
         attention.reshape(n_tp, -1, 2 * HEAD), "tp", split_axis=0, concat_axis=0, tiled=True
     )
+    ga3, gb3, y, attention = fence((ga3, gb3, y, attention))
 
     g4 = lax.ppermute(ga3, "tp", ahead)
-    y = experts(x, [ga3, gb3], [da3, db3], y)
+    y = experts(x, [ga2, gb2, ga3, gb3], [da2, db2, da3, db3], y)
     g4, d4, y, rows = fence((g4, d4, y, rows))
 
-    theirs = experts(x, [g4], [d4], y, 1, 1, False)
+    theirs = experts_last(beside, g4, d4, y, arrived.shape[0])
     extra = lax.ppermute(theirs, "tp", swap)
-    mine = experts(x, [g4], [d4], y, 0, 1, False)
+    mine = experts_last(arrived, g4, d4, y, 0)
     results = (mine.astype(F32) + extra.astype(F32)).astype(BF16).reshape(n_ep, PAD, d)
     returned = lax.all_to_all(results, "ep", split_axis=0, concat_axis=0, tiled=True)
     rows, results = fence((rows, results))

time: 214 us -> 214 us (level)
  local copies, waits for them, and re-layouts: 21.8 us -> 9.34 us
  waiting for transfers between devices: 75.3 us -> 85.2 us
  starting transfers between devices: 59.6 us -> 64.9 us
    unnamed x60 -> x33, local copies, waits for them, and re-layouts: 18.1 us -> 6.46 us
    all_to_all x1, waiting for transfers between devices: 6.48 us -> 0.01 us  [local(): lax.all_to_all(attention.reshape(n_tp, -1, 2 * HEAD), 'tp', split_axis=0,...]
    all_to_all x1, starting transfers between devices: 6.39 us -> 12.7 us  [local(): lax.all_to_all(results, 'ep', split_axis=0, concat_axis=0, tiled=True)]
    all_to_all x1, waiting for transfers between devices: 0.01 us -> 6.19 us  [local(): lax.all_to_all(outgoing, 'ep', split_axis=0, concat_axis=0, tiled=True)]
    ppermute x12, waiting for transfers between devices: 54.1 us -> 58.1 us  [ring(): return (lax.ppermute(a, 'tp', ahead), lax.ppermute(b, 'tp', back))]
    ppermute x8 -> x4, waiting for transfers between devices: 3.48 us -> 7.39 us  [the longest x3 6.06 us: across(): lax.ppermute(a, 'tp', [(2 * z + c, 2 * (z ^ bit) + c) for z, c in spot])]
    pallas_call x6 -> x5, Pallas kernels: 23.7 us -> 20 us  [the longest x2 14.3 us: experts(): pl.pallas_call(body, in_specs=[hbm] * len(args), out_specs=hbm, out_shape...]
    all_gather x1, waiting for transfers between devices: 0.01 us -> 2.96 us  [local(): kvg = lax.all_gather(packed, 'ep', axis=0)]
  transfers between devices with their start and end apart: 29 -> 25, of which waited for: 13 -> 18; matrix products, arithmetic and copies ran while one was open for 4% -> 3% of each run, Pallas kernels for 16% -> 16%
where the time goes in v1:
time: 214 us; the launch traced here: 212 us
  waiting for transfers between devices  85.2 us (40%)
  starting transfers between devices  64.9 us (30%)
  Pallas kernels  35.4 us (17%)
  between operations  14.3 us (7%)
  local copies, waits for them, and re-layouts  9.34 us (4%)
  other arithmetic  3.12 us (1%)
    ppermute x12, waiting for transfers between devices, ring(): return (lax.ppermute(a, 'tp', ahead), lax.ppermute(b, 'tp', back))  58.1 us
    ppermute x12, starting transfers between devices, ring(): return (lax.ppermute(a, 'tp', ahead), lax.ppermute(b, 'tp', back))  24.8 us
    pallas_call x2, Pallas kernels, experts(): pl.pallas_call(body, in_specs=[hbm] * len(args), out_specs=hbm, out_shape...  14.3 us
    all_to_all x1, starting transfers between devices, local(): lax.all_to_all(results, 'ep', split_axis=0, concat_axis=0, tiled=True)  12.7 us
    ppermute x3, starting transfers between devices, across(): lax.ppermute(a, 'tp', [(2 * z + c, 2 * (z ^ bit) + c) for z, c in spot])  12.2 us
    all_to_all x1, waiting for transfers between devices, local(): lax.all_to_all(results, 'ep', split_axis=0, concat_axis=0, tiled=True)  10.5 us
    pallas_call x2, Pallas kernels, attend(): pl.pallas_call(body, grid=(1,), in_specs=specs, out_specs=out_specs, out_...  7.65 us
    all_to_all x1, starting transfers between devices, local(): lax.all_to_all(outgoing, 'ep', split_axis=0, concat_axis=0, tiled=True)  7.48 us
  transfers between devices with their start and end apart: 25, of which 18 were waited for; matrix products, arithmetic and copies ran while one was open for 3% of the time, Pallas kernels for 16%

profile of v1, /device:TPU:2, one launch (start us, length us, event | category | flops | bytes accessed | tf_op | source)
XLA Modules:
  0.0 212.3 jit_solution(8585835813776476818)
XLA Ops:
  8.2 1.1 copy.20
  9.3 1.1 copy.21
  10.4 0.9 pad_maximum_fusion
  11.4 2.0 collective-permute-start
  13.4 1.8 collective-permute-done
  15.2 3.3 %collective-permute-start.17 = (bf16[128,128]{1,0:T(8,128)(2,1)S(1)}, bf16[128,128]{1,0:T(8,128)(2,1)S(1)}, u32[]{:S(2)}, u32[]{:S(2)}) collective-permute-start(bf16[128,128]{1,0:T(8,128)(2,1)S(1)} %pad_maximum_fusion.2), channel_id=1, source_target_pairs={{0,4},{1,5},{2,6},{3,7},{4,0},{5,1},{6,2},{7,3},{8,12},{9,13},{10,... | collective-permute-start | bytes 98312 | tf_op jit(solution)/shard_map/ppermute | solution.py:451
  18.5 1.9 collective-permute-done.17
  20.4 6.9 %collective-permute-start.18 = (bf16[256,128]{1,0:T(8,128)(2,1)S(1)}, bf16[256,128]{1,0:T(8,128)(2,1)S(1)}, u32[]{:S(2)}, u32[]{:S(2)}) collective-permute-start(bf16[256,128]{1,0:T(8,128)(2,1)S(1)} %constant_dynamic-update-slice_fusion.2.low_ref), channel_id=1, source_target_pairs={{0,8},{1,9},{2,10},{3,11},{4,12},{5,13},{6,14},{7,15},{8,0},{9,1},... | collective-permute-start | bytes 196616 | tf_op jit(solution)/shard_map/ppermute | solution.py:451
  27.3 2.3 %collective-permute-done.18.high_ref = bf16[256,128]{1,0:T(8,128)(2,1)S(1)} collective-permute-done((bf16[256,128]{1,0:T(8,128)(2,1)S(1)}, bf16[256,128]{1,0:T(8,128)(2,1)S(1)}, u32[]{:S(2)}, u32[]{:S(2)}) %collective-permute-start.18) | collective-permute-done | bytes 65568 | tf_op jit(solution)/shard_map/ppermute | solution.py:451
  29.8 1.3 collective-permute-done.19.far_ref
  34.4 3.6 %collective-permute-start.2 = (bf16[2,2048,128]{2,1,0:T(8,128)(2,1)}, bf16[2,2048,128]{2,1,0:T(8,128)(2,1)}, u32[]{:S(2)}, u32[]{:S(2)}) collective-permute-start(bf16[2,2048,128]{2,1,0:T(8,128)(2,1)} %constant_dynamic-update-slice_fusion.refs_2_), channel_id=1, source_target_pairs={{0,14},{1,3},{2,0},{3,5},{4,2},{5,7},{6,4},{7,9},{8,6},{9,11},{10,... | collective-permute-start | bytes 3145736 | tf_op jit(solution)/shard_map/ppermute | solution.py:448
  38.1 1.8 dispatch.1
  39.9 7.5 %all-to-all-start = ((bf16[16,16,2048]{2,1,0:T(8,128)(2,1)}), bf16[16,16,2048]{2,1,0:T(8,128)(2,1)S(1)}, u32[]{:S(2)}, u32[]{:S(2)}) async-start(bf16[16,16,2048]{2,1,0:T(8,128)(2,1)} %bitcast.5), calls=%async_computation | async-start | bytes 2097152 | tf_op jit(solution)/shard_map/all_to_all | solution.py:473
  47.5 3.2 %collective-permute-start.9 = (bf16[128,2048]{1,0:T(8,128)(2,1)S(1)}, bf16[128,2048]{1,0:T(8,128)(2,1)}, u32[]{:S(2)}, u32[]{:S(2)}) collective-permute-start(bf16[128,2048]{1,0:T(8,128)(2,1)S(1)} %bitcast.26), channel_id=1, source_target_pairs={{0,14},{1,3},{2,0},{3,5},{4,2},{5,7},{6,4},{7,9},{8,6},{9,11},{10,... | collective-permute-start | bytes 1572872 | tf_op jit(solution)/shard_map/ppermute | solution.py:448
  50.7 1.2 slice.3
  52.2 7.9 %collective-permute-done.1.refs_3_ = bf16[2,2048,128]{2,1,0:T(8,128)(2,1)} collective-permute-done((bf16[2,2048,128]{2,1,0:T(8,128)(2,1)}, bf16[2,2048,128]{2,1,0:T(8,128)(2,1)}, u32[]{:S(2)}, u32[]{:S(2)}) %collective-permute-start.1) | collective-permute-done | bytes 1048608 | tf_op jit(solution)/shard_map/ppermute | solution.py:448
  60.2 1.7 collective-permute-done.2.refs_4_
  62.5 1.3 collective-permute-start.3
  63.9 2.5 %collective-permute-start.4 = (bf16[2,2048,128]{2,1,0:T(8,128)(2,1)}, bf16[2,2048,128]{2,1,0:T(8,128)(2,1)}, u32[]{:S(2)}, u32[]{:S(2)}) collective-permute-start(bf16[2,2048,128]{2,1,0:T(8,128)(2,1)} %collective-permute-done.2.refs_4_), channel_id=1, source_target_pairs={{0,14},{1,3},{2,0},{3,5},{4,2},{5,7},{6,4},{7,9},{8,6},{9,11},{10,... | collective-permute-start | bytes 3145736 | tf_op jit(solution)/shard_map/ppermute | solution.py:448
  66.4 6.2 %all-to-all-done = bf16[16,16,2048]{2,1,0:T(8,128)(2,1)S(1)} async-done(((bf16[16,16,2048]{2,1,0:T(8,128)(2,1)}), bf16[16,16,2048]{2,1,0:T(8,128)(2,1)S(1)}, u32[]{:S(2)}, u32[]{:S(2)}) %all-to-all-start) | async-done | bytes 1048608 | tf_op jit(solution)/shard_map/all_to_all | solution.py:473
  73.0 1.4 collective-permute-start.11
  74.3 2.4 %collective-permute-start.12 = (bf16[128,2048]{1,0:T(8,128)(2,1)}, bf16[128,2048]{1,0:T(8,128)(2,1)}, u32[]{:S(2)}, u32[]{:S(2)}) collective-permute-start(bf16[128,2048]{1,0:T(8,128)(2,1)} %collective-permute-done.9.refs_7_), channel_id=1, source_target_pairs={{0,14},{1,3},{2,0},{3,5},{4,2},{5,7},{6,4},{7,9},{8,6},{9,11},{10,... | collective-permute-start | bytes 1572872 | tf_op jit(solution)/shard_map/ppermute | solution.py:448
  76.8 3.0 %all-gather.5.cloned.1.call-done = bf16[16896,128]{1,0:T(8,128)(2,1)} async-done(((bf16[1056,128]{1,0:T(8,128)(2,1)}), bf16[16896,128]{1,0:T(8,128)(2,1)}) %all-gather.5.cloned.1.call-update) | async-done | bytes 4325392 | tf_op jit(solution)/shard_map/all_gather | solution.py:465
  79.7 4.9 %attend.2 = (f32[1024,128]{1,0:T(8,128)S(1)}, f32[1024,128]{1,0:T(8,128)S(1)}) custom-call(s32[1]{0:T(128)} %bitcast.2.ep_ref, f32[1,128]{1,0:T(1,128)S(1)} %broadcast_in_dim.15.base_ref, bf16[1024,128]{1,0:T(8,128)(2,1)S(1)} %widen.1.q_ref, bf16[16,1056,128]{2,1,0:T(8,128)(2,1)} %bitcast.22), custom_call_target="tpu_custom_call" | custom-call | flops 8589934592 | bytes 4194304 | tf_op jit(solution)/shard_map/attend/pallas_call | solution.py:350
  84.6 9.3 %collective-permute-done.3.refs_2_ = bf16[2,2048,128]{2,1,0:T(8,128)(2,1)} collective-permute-done((bf16[2,2048,128]{2,1,0:T(8,128)(2,1)}, bf16[2,2048,128]{2,1,0:T(8,128)(2,1)}, u32[]{:S(2)}, u32[]{:S(2)}) %collective-permute-start.3) | collective-permute-done | bytes 1048608 | tf_op jit(solution)/shard_map/ppermute | solution.py:448
  93.9 1.7 collective-permute-done.4.refs_3_
  95.5 1.2 collective-permute-start.5
  96.8 2.4 %collective-permute-start.6 = (bf16[2,2048,128]{2,1,0:T(8,128)(2,1)}, bf16[2,2048,128]{2,1,0:T(8,128)(2,1)S(1)}, u32[]{:S(2)}, u32[]{:S(2)}) collective-permute-start(bf16[2,2048,128]{2,1,0:T(8,128)(2,1)} %collective-permute-done.4.refs_3_), channel_id=1, source_target_pairs={{0,14},{1,3},{2,0},{3,5},{4,2},{5,7},{6,4},{7,9},{8,6},{9,11},{10,... | collective-permute-start | bytes 3145736 | tf_op jit(solution)/shard_map/ppermute | solution.py:448
  99.2 5.9 %collective-permute-done.11.refs_6_ = bf16[128,2048]{1,0:T(8,128)(2,1)} collective-permute-done((bf16[128,2048]{1,0:T(8,128)(2,1)}, bf16[128,2048]{1,0:T(8,128)(2,1)}, u32[]{:S(2)}, u32[]{:S(2)}) %collective-permute-start.11) | collective-permute-done | bytes 524320 | tf_op jit(solution)/shard_map/ppermute | solution.py:448
  105.1 1.7 collective-permute-done.12.refs_7_
  106.8 3.7 %collective-permute-start.13 = (bf16[128,2048]{1,0:T(8,128)(2,1)}, bf16[128,2048]{1,0:T(8,128)(2,1)}, u32[]{:S(2)}, u32[]{:S(2)}) collective-permute-start(bf16[128,2048]{1,0:T(8,128)(2,1)} %collective-permute-done.12.refs_7_), channel_id=1, source_target_pairs={{0,14},{1,3},{2,0},{3,5},{4,2},{5,7},{6,4},{7,9},{8,6},{9,11},{10,... | collective-permute-start | bytes 1572872 | tf_op jit(solution)/shard_map/ppermute | solution.py:448
  110.5 6.7 %experts.2.refs_10_ = bf16[512,2048]{1,0:T(8,128)(2,1)} custom-call(bf16[256,2048]{1,0:T(8,128)(2,1)} %bitcast.19, bf16[256,2048]{1,0:T(8,128)(2,1)} %collective-permute-done.7.refs_1_.x_ref, bf16[2,2048,128]{2,1,0:T(8,128)(2,1)} %constant_dynamic-update-slice_fusion.refs_2_, bf16[2,2048,128]{2,1,0:T(8,128)(2,1)} %collective-permute-done.1.refs_3_, ...), custom_call_target="tpu_custom_call" | custom-call | flops 2415919104 | bytes 6291456 | tf_op jit(solution)/shard_map/experts/pallas_call | solution.py:173
  117.2 2.8 %attend.3 = bf16[512,128]{1,0:T(8,128)(2,1)} custom-call(s32[1]{0:T(128)} %bitcast.2.ep_ref, f32[1,128]{1,0:T(1,128)S(1)} %broadcast_in_dim.15.base_ref, bf16[1024,128]{1,0:T(8,128)(2,1)S(1)} %widen.1.q_ref, bf16[16,1056,128]{2,1,0:T(8,128)(2,1)} %bitcast.23, f32[1024,128]{1,0:T(8,128)S(1)} %get-tuple-element.37.rest_0_, ...), custom_call_target="tpu_custom_call" | custom-call | flops 8589934592 | bytes 4194304 | tf_op jit(solution)/shard_map/attend/pallas_call | solution.py:350
  120.0 7.5 %collective-permute-done.5.refs_4_ = bf16[2,2048,128]{2,1,0:T(8,128)(2,1)} collective-permute-done((bf16[2,2048,128]{2,1,0:T(8,128)(2,1)}, bf16[2,2048,128]{2,1,0:T(8,128)(2,1)}, u32[]{:S(2)}, u32[]{:S(2)}) %collective-permute-start.5) | collective-permute-done | bytes 1048608 | tf_op jit(solution)/shard_map/ppermute | solution.py:448
  128.4 2.1 collective-permute-start.15
  130.5 5.3 %collective-permute-done.13.refs_9_ = bf16[128,2048]{1,0:T(8,128)(2,1)} collective-permute-done((bf16[128,2048]{1,0:T(8,128)(2,1)}, bf16[128,2048]{1,0:T(8,128)(2,1)}, u32[]{:S(2)}, u32[]{:S(2)}) %collective-permute-start.13) | collective-permute-done | bytes 524320 | tf_op jit(solution)/shard_map/ppermute | solution.py:448
  135.8 3.7 %collective-permute-start.14 = (bf16[128,2048]{1,0:T(8,128)(2,1)}, bf16[128,2048]{1,0:T(8,128)(2,1)S(1)}, u32[]{:S(2)}, u32[]{:S(2)}) collective-permute-start(bf16[128,2048]{1,0:T(8,128)(2,1)} %collective-permute-done.13.refs_9_), channel_id=1, source_target_pairs={{0,14},{1,3},{2,0},{3,5},{4,2},{5,7},{6,4},{7,9},{8,6},{9,11},{10,... | collective-permute-start | bytes 1572872 | tf_op jit(solution)/shard_map/ppermute | solution.py:500
  139.5 3.7 %all-to-all-start.1 = ((bf16[16,32,128]{2,1,0:T(8,128)(2,1)}), bf16[16,32,128]{2,1,0:T(8,128)(2,1)S(1)}, u32[]{:S(2)}, u32[]{:S(2)}) async-start(bf16[16,32,128]{2,1,0:T(8,128)(2,1)} %bitcast.8), calls=%async_computation.1 | async-start | bytes 262144 | tf_op jit(solution)/shard_map/all_to_all | solution.py:502
  143.2 15.9 %collective-permute-done.15.refs_8_ = bf16[128,2048]{1,0:T(8,128)(2,1)S(1)} collective-permute-done((bf16[128,2048]{1,0:T(8,128)(2,1)}, bf16[128,2048]{1,0:T(8,128)(2,1)S(1)}, u32[]{:S(2)}, u32[]{:S(2)}) %collective-permute-start.15) | collective-permute-done | bytes 524320 | tf_op jit(solution)/shard_map/ppermute | solution.py:448
  159.9 7.5 %experts.3.y_ref = bf16[512,2048]{1,0:T(8,128)(2,1)} custom-call(bf16[256,2048]{1,0:T(8,128)(2,1)} %bitcast.20, bf16[256,2048]{1,0:T(8,128)(2,1)} %collective-permute-done.7.refs_1_.x_ref, bf16[2,2048,128]{2,1,0:T(8,128)(2,1)} %collective-permute-done.3.refs_2_, bf16[2,2048,128]{2,1,0:T(8,128)(2,1)} %collective-permute-done.4.refs_3_, ...), custom_call_target="tpu_custom_call" | custom-call | flops 3221225472 | bytes 6291456 | tf_op jit(solution)/shard_map/experts/pallas_call | solution.py:173
  167.5 2.8 %experts_last.3 = bf16[256,2048]{1,0:T(8,128)(2,1)S(1)} custom-call(bf16[256,2048]{1,0:T(8,128)(2,1)} %collective-permute-done.7.refs_1_.x_ref, bf16[2,2048,128]{2,1,0:T(8,128)(2,1)S(1)} %collective-permute-done.10.gu_ref, bf16[128,2048]{1,0:T(8,128)(2,1)S(1)} %collective-permute-done.14.d_ref, bf16[512,2048]{1,0:T(8,128)(2,1)} %experts.3.y_ref), custom_call_target="tpu_custom_call" | custom-call | flops 402653184 | bytes 5242880 | tf_op jit(solution)/shard_map/experts_last/pallas_call | solution.py:210
  170.4 2.8 %experts_last.2 = bf16[256,2048]{1,0:T(8,128)(2,1)S(1)} custom-call(bf16[256,2048]{1,0:T(8,128)(2,1)} %bitcast.21, bf16[2,2048,128]{2,1,0:T(8,128)(2,1)S(1)} %collective-permute-done.10.gu_ref, bf16[128,2048]{1,0:T(8,128)(2,1)S(1)} %collective-permute-done.14.d_ref, bf16[512,2048]{1,0:T(8,128)(2,1)} %experts.3.y_ref), custom_call_target="tpu_custom_call" | custom-call | flops 402653184 | bytes 5242880 | tf_op jit(solution)/shard_map/experts_last/pallas_call | solution.py:210
  173.3 1.4 add_convert_fusion
  174.7 12.7 %all-to-all-start.2 = ((bf16[16,16,2048]{2,1,0:T(8,128)(2,1)}), bf16[16,16,2048]{2,1,0:T(8,128)(2,1)S(1)}, u32[]{:S(2)}, u32[]{:S(2)}) async-start(bf16[16,16,2048]{2,1,0:T(8,128)(2,1)} %bitcast.9), calls=%async_computation.2 | async-start | bytes 2097152 | tf_op jit(solution)/shard_map/all_to_all | solution.py:515
  187.5 2.2 %copy-done.1 = bf16[16384,128]{1,0:T(8,128)(2,1)S(1)} copy-done((bf16[16384,128]{1,0:T(8,128)(2,1)S(1)}, bf16[16384,128]{1,0:T(8,128)(2,1)}, u32[]{:S(2)}) %copy-start.1) | copy-done | bytes 4194328
  189.7 3.6 %project.1 = bf16[64,2048]{1,0:T(8,128)(2,1)} custom-call(bf16[16,32,128]{2,1,0:T(8,128)(2,1)S(1)} %all-to-all-done.1.a_ref, bf16[16,1024,128]{2,1,0:T(8,128)(2,1)S(1)} %bitcast.15), custom_call_target="tpu_custom_call" | custom-call | tf_op jit(solution)/shard_map/project/pallas_call | solution.py:411
  193.3 10.5 %all-to-all-done.2 = bf16[16,16,2048]{2,1,0:T(8,128)(2,1)S(1)} async-done(((bf16[16,16,2048]{2,1,0:T(8,128)(2,1)}), bf16[16,16,2048]{2,1,0:T(8,128)(2,1)S(1)}, u32[]{:S(2)}, u32[]{:S(2)}) %all-to-all-start.2) | async-done | bytes 1048608 | tf_op jit(solution)/shard_map/all_to_all | solution.py:515
  203.8 1.6 combine.1
  (61 shorter events, 7.8 us)
Async XLA Ops:
  7.2 4.2 %copy-start = (bf16[64,2048]{1,0:T(8,128)(2,1)S(1)}, bf16[64,2048]{1,0:T(8,128)(2,1)}, u32[]{:S(2)}) copy-start(bf16[64,2048]{1,0:T(8,128)(2,1)} %param.16) | copy-start | bytes 786436
  7.2 24.7 %copy-start.7 = (bf16[1,2048,128]{2,1,0:T(8,128)(2,1)S(1)}, bf16[1,2048,128]{2,1,0:T(8,128)(2,1)}, u32[]{:S(2)}) copy-start(bf16[1,2048,128]{2,1,0:T(8,128)(2,1)} %param.19) | copy-start | bytes 1572868
  7.2 72.5 %all-gather.5.cloned.1.call-start = ((), (), s32[]{:S(2)}) async-start(), calls=%async_computation.3 | async-start | bytes 4595712 | tf_op jit(solution)/shard_map/all_gather | solution.py:465
  8.2 24.6 %copy-start.8 = (bf16[1,2048,128]{2,1,0:T(8,128)(2,1)S(1)}, bf16[1,2048,128]{2,1,0:T(8,128)(2,1)}, u32[]{:S(2)}) copy-start(bf16[1,2048,128]{2,1,0:T(8,128)(2,1)} %param.20) | copy-start | bytes 1572868
  10.4 27.6 %copy-start.10 = (s32[96,2]{0,1:T(2,128)S(1)}, s32[96,2]{0,1:T(2,128)}, u32[]{:S(2)}) copy-start(s32[96,2]{0,1:T(2,128)} %param.22) | copy-start | bytes 2308
  10.4 27.7 %copy-start.2 = (bf16[96,2048]{1,0:T(8,128)(2,1)S(1)}, bf16[96,2048]{1,0:T(8,128)(2,1)}, u32[]{:S(2)}) copy-start(bf16[96,2048]{1,0:T(8,128)(2,1)} %tokens_ref.1) | copy-start | bytes 1179652
  10.4 27.7 %copy-start.3 = (f32[2048]{0:T(1024)S(1)}, f32[2048]{0:T(1024)}, u32[]{:S(2)}) copy-start(f32[2048]{0:T(1024)} %param.18) | copy-start | bytes 24580
  11.3 176.2 %all-gather.7.cloned.1.call-start = ((), (), s32[]{:S(2)}) async-start(), calls=%async_computation.4 | async-start | bytes 4456448 | tf_op jit(solution)/shard_map/all_gather | solution.py:487
  11.4 3.8 %collective-permute-start = (bf16[64,128]{1,0:T(8,128)(2,1)S(1)}, bf16[64,128]{1,0:T(8,128)(2,1)S(1)}, u32[]{:S(2)}, u32[]{:S(2)}) collective-permute-start(bf16[64,128]{1,0:T(8,128)(2,1)S(1)} %constant_dynamic-slice_fusion), channel_id=1, source_target_pairs={{0,2},{1,3},{2,0},{3,1},{4,6},{5,7},{6,4},{7,5},{8,10},{9,11},{10,... | collective-permute-start | bytes 49160 | tf_op jit(solution)/shard_map/ppermute | solution.py:451
  15.2 5.2 %collective-permute-start.17 = (bf16[128,128]{1,0:T(8,128)(2,1)S(1)}, bf16[128,128]{1,0:T(8,128)(2,1)S(1)}, u32[]{:S(2)}, u32[]{:S(2)}) collective-permute-start(bf16[128,128]{1,0:T(8,128)(2,1)S(1)} %pad_maximum_fusion.2), channel_id=1, source_target_pairs={{0,4},{1,5},{2,6},{3,7},{4,0},{5,1},{6,2},{7,3},{8,12},{9,13},{10,... | collective-permute-start | bytes 98312 | tf_op jit(solution)/shard_map/ppermute | solution.py:451
  20.4 9.3 %collective-permute-start.18 = (bf16[256,128]{1,0:T(8,128)(2,1)S(1)}, bf16[256,128]{1,0:T(8,128)(2,1)S(1)}, u32[]{:S(2)}, u32[]{:S(2)}) collective-permute-start(bf16[256,128]{1,0:T(8,128)(2,1)S(1)} %constant_dynamic-update-slice_fusion.2.low_ref), channel_id=1, source_target_pairs={{0,8},{1,9},{2,10},{3,11},{4,12},{5,13},{6,14},{7,15},{8,0},{9,1},... | collective-permute-start | bytes 196616 | tf_op jit(solution)/shard_map/ppermute | solution.py:451
  29.7 1.4 collective-permute-start.19
  32.7 14.7 %copy-start.12 = (bf16[1,128,2048]{2,1,0:T(8,128)(2,1)S(1)}, bf16[1,128,2048]{2,1,0:T(8,128)(2,1)}, u32[]{:S(2)}) copy-start(bf16[1,128,2048]{2,1,0:T(8,128)(2,1)} %param.21) | copy-start | bytes 1572868
  32.7 19.2 %copy-start.9 = (bf16[1024,64]{0,1:T(8,128)(2,1)S(1)}, bf16[1024,64]{0,1:T(8,128)(2,1)}, u32[]{:S(2)}) copy-start(bf16[1024,64]{0,1:T(8,128)(2,1)} %param.12) | copy-start | bytes 393220
  33.6 26.6 %collective-permute-start.1 = (bf16[2,2048,128]{2,1,0:T(8,128)(2,1)}, bf16[2,2048,128]{2,1,0:T(8,128)(2,1)}, u32[]{:S(2)}, u32[]{:S(2)}) collective-permute-start(bf16[2,2048,128]{2,1,0:T(8,128)(2,1)} %constant_dynamic-update-slice_fusion.refs_2_), channel_id=1, source_target_pairs={{0,2},{1,15},{2,4},{3,1},{4,6},{5,3},{6,8},{7,5},{8,10},{9,7},{10,... | collective-permute-start | bytes 3145736 | tf_op jit(solution)/shard_map/ppermute | solution.py:448
  34.4 27.5 %collective-permute-start.2 = (bf16[2,2048,128]{2,1,0:T(8,128)(2,1)}, bf16[2,2048,128]{2,1,0:T(8,128)(2,1)}, u32[]{:S(2)}, u32[]{:S(2)}) collective-permute-start(bf16[2,2048,128]{2,1,0:T(8,128)(2,1)} %constant_dynamic-update-slice_fusion.refs_2_), channel_id=1, source_target_pairs={{0,14},{1,3},{2,0},{3,5},{4,2},{5,7},{6,4},{7,9},{8,6},{9,11},{10,... | collective-permute-start | bytes 3145736 | tf_op jit(solution)/shard_map/ppermute | solution.py:448
  39.9 32.7 %all-to-all-start = ((bf16[16,16,2048]{2,1,0:T(8,128)(2,1)}), bf16[16,16,2048]{2,1,0:T(8,128)(2,1)S(1)}, u32[]{:S(2)}, u32[]{:S(2)}) async-start(bf16[16,16,2048]{2,1,0:T(8,128)(2,1)} %bitcast.5), calls=%async_computation | async-start | bytes 2097152 | tf_op jit(solution)/shard_map/all_to_all | solution.py:473
  47.4 25.2 %collective-permute-start.8 = (bf16[128,2048]{1,0:T(8,128)(2,1)S(1)}, bf16[128,2048]{1,0:T(8,128)(2,1)}, u32[]{:S(2)}, u32[]{:S(2)}) collective-permute-start(bf16[128,2048]{1,0:T(8,128)(2,1)S(1)} %bitcast.25), channel_id=1, source_target_pairs={{0,2},{1,15},{2,4},{3,1},{4,6},{5,3},{6,8},{7,5},{8,10},{9,7},{10,... | collective-permute-start | bytes 1572872 | tf_op jit(solution)/shard_map/ppermute | solution.py:448
  47.5 25.5 %collective-permute-start.9 = (bf16[128,2048]{1,0:T(8,128)(2,1)S(1)}, bf16[128,2048]{1,0:T(8,128)(2,1)}, u32[]{:S(2)}, u32[]{:S(2)}) collective-permute-start(bf16[128,2048]{1,0:T(8,128)(2,1)S(1)} %bitcast.26), channel_id=1, source_target_pairs={{0,14},{1,3},{2,0},{3,5},{4,2},{5,7},{6,4},{7,9},{8,6},{9,11},{10,... | collective-permute-start | bytes 1572872 | tf_op jit(solution)/shard_map/ppermute | solution.py:448
  62.5 31.3 %collective-permute-start.3 = (bf16[2,2048,128]{2,1,0:T(8,128)(2,1)}, bf16[2,2048,128]{2,1,0:T(8,128)(2,1)}, u32[]{:S(2)}, u32[]{:S(2)}) collective-permute-start(bf16[2,2048,128]{2,1,0:T(8,128)(2,1)} %collective-permute-done.1.refs_3_), channel_id=1, source_target_pairs={{0,2},{1,15},{2,4},{3,1},{4,6},{5,3},{6,8},{7,5},{8,10},{9,7},{10,... | collective-permute-start | bytes 3145736 | tf_op jit(solution)/shard_map/ppermute | solution.py:448
  63.9 31.7 %collective-permute-start.4 = (bf16[2,2048,128]{2,1,0:T(8,128)(2,1)}, bf16[2,2048,128]{2,1,0:T(8,128)(2,1)}, u32[]{:S(2)}, u32[]{:S(2)}) collective-permute-start(bf16[2,2048,128]{2,1,0:T(8,128)(2,1)} %collective-permute-done.2.refs_4_), channel_id=1, source_target_pairs={{0,14},{1,3},{2,0},{3,5},{4,2},{5,7},{6,4},{7,9},{8,6},{9,11},{10,... | collective-permute-start | bytes 3145736 | tf_op jit(solution)/shard_map/ppermute | solution.py:448
  72.6 12.0 %copy-start.4 = (bf16[16,16,2048]{2,1,0:T(8,128)(2,1)}, bf16[16,16,2048]{2,1,0:T(8,128)(2,1)S(1)}, u32[]{:S(2)}) copy-start(bf16[16,16,2048]{2,1,0:T(8,128)(2,1)S(1)} %all-to-all-done) | copy-start | bytes 3145732
  72.6 37.9 %collective-permute-start.7 = (bf16[256,2048]{1,0:T(8,128)(2,1)S(1)}, bf16[256,2048]{1,0:T(8,128)(2,1)}, u32[]{:S(2)}, u32[]{:S(2)}) collective-permute-start(bf16[256,2048]{1,0:T(8,128)(2,1)S(1)} %bitcast.18), channel_id=1, source_target_pairs={{0,1},{1,0},{2,3},{3,2},{4,5},{5,4},{6,7},{7,6},{8,9},{9,8},{10,11... | collective-permute-start | bytes 3145736 | tf_op jit(solution)/shard_map/ppermute | solution.py:489
  73.0 32.1 %collective-permute-start.11 = (bf16[128,2048]{1,0:T(8,128)(2,1)}, bf16[128,2048]{1,0:T(8,128)(2,1)}, u32[]{:S(2)}, u32[]{:S(2)}) collective-permute-start(bf16[128,2048]{1,0:T(8,128)(2,1)} %collective-permute-done.8.refs_6_), channel_id=1, source_target_pairs={{0,2},{1,15},{2,4},{3,1},{4,6},{5,3},{6,8},{7,5},{8,10},{9,7},{10,... | collective-permute-start | bytes 1572872 | tf_op jit(solution)/shard_map/ppermute | solution.py:448
  74.3 32.5 %collective-permute-start.12 = (bf16[128,2048]{1,0:T(8,128)(2,1)}, bf16[128,2048]{1,0:T(8,128)(2,1)}, u32[]{:S(2)}, u32[]{:S(2)}) collective-permute-start(bf16[128,2048]{1,0:T(8,128)(2,1)} %collective-permute-done.9.refs_7_), channel_id=1, source_target_pairs={{0,14},{1,3},{2,0},{3,5},{4,2},{5,7},{6,4},{7,9},{8,6},{9,11},{10,... | collective-permute-start | bytes 1572872 | tf_op jit(solution)/shard_map/ppermute | solution.py:448
  95.5 32.0 %collective-permute-start.5 = (bf16[2,2048,128]{2,1,0:T(8,128)(2,1)}, bf16[2,2048,128]{2,1,0:T(8,128)(2,1)}, u32[]{:S(2)}, u32[]{:S(2)}) collective-permute-start(bf16[2,2048,128]{2,1,0:T(8,128)(2,1)} %collective-permute-done.3.refs_2_), channel_id=1, source_target_pairs={{0,2},{1,15},{2,4},{3,1},{4,6},{5,3},{6,8},{7,5},{8,10},{9,7},{10,... | collective-permute-start | bytes 3145736 | tf_op jit(solution)/shard_map/ppermute | solution.py:448
  96.8 31.6 %collective-permute-start.6 = (bf16[2,2048,128]{2,1,0:T(8,128)(2,1)}, bf16[2,2048,128]{2,1,0:T(8,128)(2,1)S(1)}, u32[]{:S(2)}, u32[]{:S(2)}) collective-permute-start(bf16[2,2048,128]{2,1,0:T(8,128)(2,1)} %collective-permute-done.4.refs_3_), channel_id=1, source_target_pairs={{0,14},{1,3},{2,0},{3,5},{4,2},{5,7},{6,4},{7,9},{8,6},{9,11},{10,... | collective-permute-start | bytes 3145736 | tf_op jit(solution)/shard_map/ppermute | solution.py:448
  106.8 29.0 %collective-permute-start.13 = (bf16[128,2048]{1,0:T(8,128)(2,1)}, bf16[128,2048]{1,0:T(8,128)(2,1)}, u32[]{:S(2)}, u32[]{:S(2)}) collective-permute-start(bf16[128,2048]{1,0:T(8,128)(2,1)} %collective-permute-done.12.refs_7_), channel_id=1, source_target_pairs={{0,14},{1,3},{2,0},{3,5},{4,2},{5,7},{6,4},{7,9},{8,6},{9,11},{10,... | collective-permute-start | bytes 1572872 | tf_op jit(solution)/shard_map/ppermute | solution.py:448
  128.4 2.1 copy-start.5
  128.4 39.0 %collective-permute-start.10 = (bf16[2,2048,128]{2,1,0:T(8,128)(2,1)}, bf16[2,2048,128]{2,1,0:T(8,128)(2,1)S(1)}, u32[]{:S(2)}, u32[]{:S(2)}) collective-permute-start(bf16[2,2048,128]{2,1,0:T(8,128)(2,1)} %collective-permute-done.5.refs_4_), channel_id=1, source_target_pairs={{0,2},{1,15},{2,4},{3,1},{4,6},{5,3},{6,8},{7,5},{8,10},{9,7},{10,... | collective-permute-start | bytes 3145736 | tf_op jit(solution)/shard_map/ppermute | solution.py:507
  128.4 30.7 %collective-permute-start.15 = (bf16[128,2048]{1,0:T(8,128)(2,1)}, bf16[128,2048]{1,0:T(8,128)(2,1)S(1)}, u32[]{:S(2)}, u32[]{:S(2)}) collective-permute-start(bf16[128,2048]{1,0:T(8,128)(2,1)} %collective-permute-done.11.refs_6_), channel_id=1, source_target_pairs={{0,2},{1,15},{2,4},{3,1},{4,6},{5,3},{6,8},{7,5},{8,10},{9,7},{10,... | collective-permute-start | bytes 1572872 | tf_op jit(solution)/shard_map/ppermute | solution.py:448
  135.8 31.6 %collective-permute-start.14 = (bf16[128,2048]{1,0:T(8,128)(2,1)}, bf16[128,2048]{1,0:T(8,128)(2,1)S(1)}, u32[]{:S(2)}, u32[]{:S(2)}) collective-permute-start(bf16[128,2048]{1,0:T(8,128)(2,1)} %collective-permute-done.13.refs_9_), channel_id=1, source_target_pairs={{0,14},{1,3},{2,0},{3,5},{4,2},{5,7},{6,4},{7,9},{8,6},{9,11},{10,... | collective-permute-start | bytes 1572872 | tf_op jit(solution)/shard_map/ppermute | solution.py:500
  139.5 27.9 %all-to-all-start.1 = ((bf16[16,32,128]{2,1,0:T(8,128)(2,1)}), bf16[16,32,128]{2,1,0:T(8,128)(2,1)S(1)}, u32[]{:S(2)}, u32[]{:S(2)}) async-start(bf16[16,32,128]{2,1,0:T(8,128)(2,1)} %bitcast.8), calls=%async_computation.1 | async-start | bytes 262144 | tf_op jit(solution)/shard_map/all_to_all | solution.py:502
  159.1 0.8 copy-start.6
  170.3 3.0 %collective-permute-start.16 = (bf16[256,2048]{1,0:T(8,128)(2,1)S(1)}, bf16[256,2048]{1,0:T(8,128)(2,1)S(1)}, u32[]{:S(2)}, u32[]{:S(2)}) collective-permute-start(bf16[256,2048]{1,0:T(8,128)(2,1)S(1)} %experts_last.3), channel_id=1, source_target_pairs={{0,1},{1,0},{2,3},{3,2},{4,5},{5,4},{6,7},{7,6},{8,9},{9,8},{10,11... | collective-permute-start | bytes 3145736 | tf_op jit(solution)/shard_map/ppermute | solution.py:512
  173.2 14.2 %copy-start.11 = (f32[96,2]{0,1:T(2,128)S(1)}, f32[96,2]{0,1:T(2,128)}, u32[]{:S(2)}) copy-start(f32[96,2]{0,1:T(2,128)} %param.23) | copy-start | bytes 2308
  174.7 29.2 %all-to-all-start.2 = ((bf16[16,16,2048]{2,1,0:T(8,128)(2,1)}), bf16[16,16,2048]{2,1,0:T(8,128)(2,1)S(1)}, u32[]{:S(2)}, u32[]{:S(2)}) async-start(bf16[16,16,2048]{2,1,0:T(8,128)(2,1)} %bitcast.9), calls=%async_computation.2 | async-start | bytes 2097152 | tf_op jit(solution)/shard_map/all_to_all | solution.py:515
  187.5 2.2 %copy-start.1 = (bf16[16384,128]{1,0:T(8,128)(2,1)S(1)}, bf16[16384,128]{1,0:T(8,128)(2,1)}, u32[]{:S(2)}) copy-start(bf16[16384,128]{1,0:T(8,128)(2,1)} %all-gather.7.cloned.1.call-done) | copy-start | bytes 12582916
Sparse Core Ops, SparseCore 0:
  11.4 68.2 all-gather.4
  82.7 53.5 all-gather.6

commit v2 on v1

--- a/solution.py
+++ b/solution.py
@@ -69,27 +69,38 @@
     )(tokens, gain, choice)
 
 
-def combine_body(own_ref, choice_ref, weight_ref, out_ref):
+def mix_body(choice_ref, weight_ref, high_ref, low_ref):
     slot0, slot1 = slots_of(choice_ref[...])
     w = weight_ref[...]
     lane = lax.broadcasted_iota(jnp.int32, (w.shape[0], EXPERTS * PAD), 1)
     mix = jnp.where(lane == slot0, w[:, 0:1], 0.0) + jnp.where(lane == slot1, w[:, 1:2], 0.0)
     high = mix.astype(BF16)
-    low = (mix - high.astype(F32)).astype(BF16)
-    rows = own_ref[...]
+    high_ref[...] = high
+    low_ref[...] = (mix - high.astype(F32)).astype(BF16)
+
+
+def mixing(choice, weights):
+    part = jax.ShapeDtypeStruct((choice.shape[0], EXPERTS * PAD), BF16)
+    return pl.pallas_call(
+        mix_body, out_shape=(part, part), compiler_params=params(), name="mixing"
+    )(choice, weights)
+
+
+def combine_body(rows_ref, high_ref, low_ref, out_ref):
+    rows = rows_ref[...]
     out_ref[...] = (
-        jnp.dot(high, rows, preferred_element_type=F32)
-        + jnp.dot(low, rows, preferred_element_type=F32)
+        jnp.dot(high_ref[...], rows, preferred_element_type=F32)
+        + jnp.dot(low_ref[...], rows, preferred_element_type=F32)
     ).astype(BF16)
 
 
-def combine(returned, choice, weights):
+def combine(returned, high, low):
     return pl.pallas_call(
         combine_body,
-        out_shape=jax.ShapeDtypeStruct((choice.shape[0], returned.shape[1]), BF16),
+        out_shape=jax.ShapeDtypeStruct((high.shape[0], returned.shape[1]), BF16),
         compiler_params=params(),
         name="combine",
-    )(returned, choice, weights)
+    )(returned, high, low)
 
 
 def gated(gate_pre, up_pre):
@@ -502,11 +513,12 @@
     rows = lax.all_to_all(
         attention.reshape(n_tp, -1, 2 * HEAD), "tp", split_axis=0, concat_axis=0, tiled=True
     )
+    mixed = mixing(expert_choice, route_weights)
     ga3, gb3, y, attention = fence((ga3, gb3, y, attention))
 
     g4 = lax.ppermute(ga3, "tp", ahead)
     y = experts(x, [ga2, gb2, ga3, gb3], [da2, db2, da3, db3], y)
-    g4, d4, y, rows = fence((g4, d4, y, rows))
+    g4, d4, y = fence((g4, d4, y))
 
     theirs = experts_last(beside, g4, d4, y, arrived.shape[0])
     extra = lax.ppermute(theirs, "tp", swap)
@@ -515,7 +527,7 @@
     returned = lax.all_to_all(results, "ep", split_axis=0, concat_axis=0, tiled=True)
     rows, results = fence((rows, results))
     mixer_output = project(rows, columns)
-    expert_output = combine(returned.reshape(n_ep * PAD, d), expert_choice, route_weights)
+    expert_output = combine(returned.reshape(n_ep * PAD, d), *mixed)
     return (mixer_output, expert_output)
 
 

time: 214 us -> 222 us (1.037)
  waiting for transfers between devices: 85.2 us -> 90.6 us
    all_to_all x1, waiting for transfers between devices: 0.01 us -> 3.17 us  [local(): lax.all_to_all(attention.reshape(n_tp, -1, 2 * HEAD), 'tp', split_axis=0,...]
    ppermute x12, waiting for transfers between devices: 58.1 us -> 60.5 us  [ring(): return (lax.ppermute(a, 'tp', ahead), lax.ppermute(b, 'tp', back))]
    unnamed x33 -> x37, local copies, waits for them, and re-layouts: 6.46 us -> 6.47 us
  transfers between devices with their start and end apart: 25 -> 25, of which waited for: 18 -> 19; matrix products, arithmetic and copies ran while one was open for 3% -> 3% of each run, Pallas kernels for 16% -> 16%
where the time goes in v2:
time: 222 us; the launch traced here: 219 us
  waiting for transfers between devices  90.6 us (41%)
  starting transfers between devices  64.8 us (29%)
  Pallas kernels  35.4 us (16%)
  between operations  14.4 us (6%)
  local copies, waits for them, and re-layouts  9.29 us (4%)
  other arithmetic  4.32 us (2%)
    ppermute x12, waiting for transfers between devices, ring(): return (lax.ppermute(a, 'tp', ahead), lax.ppermute(b, 'tp', back))  60.5 us
    ppermute x12, starting transfers between devices, ring(): return (lax.ppermute(a, 'tp', ahead), lax.ppermute(b, 'tp', back))  24.8 us
    pallas_call x2, Pallas kernels, experts(): pl.pallas_call(body, in_specs=[hbm] * len(args), out_specs=hbm, out_shape...  14.2 us
    ppermute x3, starting transfers between devices, across(): lax.ppermute(a, 'tp', [(2 * z + c, 2 * (z ^ bit) + c) for z, c in spot])  12.2 us
    all_to_all x1, starting transfers between devices, local(): lax.all_to_all(results, 'ep', split_axis=0, concat_axis=0, tiled=True)  10.9 us
    all_to_all x1, waiting for transfers between devices, local(): lax.all_to_all(results, 'ep', split_axis=0, concat_axis=0, tiled=True)  10.3 us
    pallas_call x2, Pallas kernels, attend(): pl.pallas_call(body, grid=(1,), in_specs=specs, out_specs=out_specs, out_...  7.65 us
    all_to_all x1, starting transfers between devices, local(): lax.all_to_all(outgoing, 'ep', split_axis=0, concat_axis=0, tiled=True)  7.48 us
  transfers between devices with their start and end apart: 25, of which 19 were waited for; matrix products, arithmetic and copies ran while one was open for 3% of the time, Pallas kernels for 16%

profile of v2, /device:TPU:2, one launch (start us, length us, event | category | flops | bytes accessed | tf_op | source)
XLA Modules:
  0.0 218.8 jit_solution(13167988355824843168)
XLA Ops:
  8.2 1.1 copy.21
  9.3 1.1 copy.20
  11.4 2.0 collective-permute-start
  13.4 1.8 collective-permute-done
  15.2 3.3 %collective-permute-start.17 = (bf16[128,128]{1,0:T(8,128)(2,1)S(1)}, bf16[128,128]{1,0:T(8,128)(2,1)S(1)}, u32[]{:S(2)}, u32[]{:S(2)}) collective-permute-start(bf16[128,128]{1,0:T(8,128)(2,1)S(1)} %pad_maximum_fusion.2), channel_id=1, source_target_pairs={{0,4},{1,5},{2,6},{3,7},{4,0},{5,1},{6,2},{7,3},{8,12},{9,13},{10,... | collective-permute-start | bytes 98312 | tf_op jit(solution)/shard_map/ppermute | solution.py:462
  18.5 1.9 collective-permute-done.17
  20.4 6.9 %collective-permute-start.18 = (bf16[256,128]{1,0:T(8,128)(2,1)S(1)}, bf16[256,128]{1,0:T(8,128)(2,1)S(1)}, u32[]{:S(2)}, u32[]{:S(2)}) collective-permute-start(bf16[256,128]{1,0:T(8,128)(2,1)S(1)} %constant_dynamic-update-slice_fusion.2.low_ref), channel_id=1, source_target_pairs={{0,8},{1,9},{2,10},{3,11},{4,12},{5,13},{6,14},{7,15},{8,0},{9,1},... | collective-permute-start | bytes 196616 | tf_op jit(solution)/shard_map/ppermute | solution.py:462
  27.3 2.3 %collective-permute-done.18.high_ref = bf16[256,128]{1,0:T(8,128)(2,1)S(1)} collective-permute-done((bf16[256,128]{1,0:T(8,128)(2,1)S(1)}, bf16[256,128]{1,0:T(8,128)(2,1)S(1)}, u32[]{:S(2)}, u32[]{:S(2)}) %collective-permute-start.18) | collective-permute-done | bytes 65568 | tf_op jit(solution)/shard_map/ppermute | solution.py:462
  29.8 1.3 collective-permute-done.19.far_ref
  34.4 3.6 %collective-permute-start.2 = (bf16[2,2048,128]{2,1,0:T(8,128)(2,1)}, bf16[2,2048,128]{2,1,0:T(8,128)(2,1)}, u32[]{:S(2)}, u32[]{:S(2)}) collective-permute-start(bf16[2,2048,128]{2,1,0:T(8,128)(2,1)} %constant_dynamic-update-slice_fusion.refs_2_), channel_id=1, source_target_pairs={{0,14},{1,3},{2,0},{3,5},{4,2},{5,7},{6,4},{7,9},{8,6},{9,11},{10,... | collective-permute-start | bytes 3145736 | tf_op jit(solution)/shard_map/ppermute | solution.py:459
  38.1 1.8 dispatch.1
  39.9 7.5 %all-to-all-start.1 = ((bf16[16,16,2048]{2,1,0:T(8,128)(2,1)}), bf16[16,16,2048]{2,1,0:T(8,128)(2,1)S(1)}, u32[]{:S(2)}, u32[]{:S(2)}) async-start(bf16[16,16,2048]{2,1,0:T(8,128)(2,1)} %bitcast.6), calls=%async_computation.1 | async-start | bytes 2097152 | tf_op jit(solution)/shard_map/all_to_all | solution.py:484
  47.5 3.2 %collective-permute-start.9 = (bf16[128,2048]{1,0:T(8,128)(2,1)S(1)}, bf16[128,2048]{1,0:T(8,128)(2,1)}, u32[]{:S(2)}, u32[]{:S(2)}) collective-permute-start(bf16[128,2048]{1,0:T(8,128)(2,1)S(1)} %bitcast.26), channel_id=1, source_target_pairs={{0,14},{1,3},{2,0},{3,5},{4,2},{5,7},{6,4},{7,9},{8,6},{9,11},{10,... | collective-permute-start | bytes 1572872 | tf_op jit(solution)/shard_map/ppermute | solution.py:459
  50.7 1.2 slice.3
  52.2 8.0 %collective-permute-done.1.refs_3_ = bf16[2,2048,128]{2,1,0:T(8,128)(2,1)} collective-permute-done((bf16[2,2048,128]{2,1,0:T(8,128)(2,1)}, bf16[2,2048,128]{2,1,0:T(8,128)(2,1)}, u32[]{:S(2)}, u32[]{:S(2)}) %collective-permute-start.1) | collective-permute-done | bytes 1048608 | tf_op jit(solution)/shard_map/ppermute | solution.py:459
  60.2 1.7 collective-permute-done.2.refs_4_
  62.5 1.3 collective-permute-start.3
  63.8 2.5 %collective-permute-start.4 = (bf16[2,2048,128]{2,1,0:T(8,128)(2,1)}, bf16[2,2048,128]{2,1,0:T(8,128)(2,1)}, u32[]{:S(2)}, u32[]{:S(2)}) collective-permute-start(bf16[2,2048,128]{2,1,0:T(8,128)(2,1)} %collective-permute-done.2.refs_4_), channel_id=1, source_target_pairs={{0,14},{1,3},{2,0},{3,5},{4,2},{5,7},{6,4},{7,9},{8,6},{9,11},{10,... | collective-permute-start | bytes 3145736 | tf_op jit(solution)/shard_map/ppermute | solution.py:459
  66.4 6.3 %all-to-all-done.1 = bf16[16,16,2048]{2,1,0:T(8,128)(2,1)S(1)} async-done(((bf16[16,16,2048]{2,1,0:T(8,128)(2,1)}), bf16[16,16,2048]{2,1,0:T(8,128)(2,1)S(1)}, u32[]{:S(2)}, u32[]{:S(2)}) %all-to-all-start.1) | async-done | bytes 1048608 | tf_op jit(solution)/shard_map/all_to_all | solution.py:484
  73.0 1.4 collective-permute-start.11
  74.3 2.4 %collective-permute-start.12 = (bf16[128,2048]{1,0:T(8,128)(2,1)}, bf16[128,2048]{1,0:T(8,128)(2,1)}, u32[]{:S(2)}, u32[]{:S(2)}) collective-permute-start(bf16[128,2048]{1,0:T(8,128)(2,1)} %collective-permute-done.9.refs_7_), channel_id=1, source_target_pairs={{0,14},{1,3},{2,0},{3,5},{4,2},{5,7},{6,4},{7,9},{8,6},{9,11},{10,... | collective-permute-start | bytes 1572872 | tf_op jit(solution)/shard_map/ppermute | solution.py:459
  76.8 3.0 %all-gather.5.cloned.1.call-done = bf16[16896,128]{1,0:T(8,128)(2,1)} async-done(((bf16[1056,128]{1,0:T(8,128)(2,1)}), bf16[16896,128]{1,0:T(8,128)(2,1)}) %all-gather.5.cloned.1.call-update) | async-done | bytes 4325392 | tf_op jit(solution)/shard_map/all_gather | solution.py:476
  79.7 4.8 %attend.2 = (f32[1024,128]{1,0:T(8,128)S(1)}, f32[1024,128]{1,0:T(8,128)S(1)}) custom-call(s32[1]{0:T(128)} %bitcast.ep_ref, f32[1,128]{1,0:T(1,128)S(1)} %broadcast_in_dim.15.base_ref, bf16[1024,128]{1,0:T(8,128)(2,1)S(1)} %widen.1.q_ref, bf16[16,1056,128]{2,1,0:T(8,128)(2,1)} %bitcast.22), custom_call_target="tpu_custom_call" | custom-call | flops 8589934592 | bytes 4194304 | tf_op jit(solution)/shard_map/attend/pallas_call | solution.py:361
  84.6 9.3 %collective-permute-done.3.refs_2_ = bf16[2,2048,128]{2,1,0:T(8,128)(2,1)} collective-permute-done((bf16[2,2048,128]{2,1,0:T(8,128)(2,1)}, bf16[2,2048,128]{2,1,0:T(8,128)(2,1)}, u32[]{:S(2)}, u32[]{:S(2)}) %collective-permute-start.3) | collective-permute-done | bytes 1048608 | tf_op jit(solution)/shard_map/ppermute | solution.py:459
  93.9 1.7 collective-permute-done.4.refs_3_
  95.6 1.2 collective-permute-start.5
  96.8 2.4 %collective-permute-start.6 = (bf16[2,2048,128]{2,1,0:T(8,128)(2,1)}, bf16[2,2048,128]{2,1,0:T(8,128)(2,1)S(1)}, u32[]{:S(2)}, u32[]{:S(2)}) collective-permute-start(bf16[2,2048,128]{2,1,0:T(8,128)(2,1)} %collective-permute-done.4.refs_3_), channel_id=1, source_target_pairs={{0,14},{1,3},{2,0},{3,5},{4,2},{5,7},{6,4},{7,9},{8,6},{9,11},{10,... | collective-permute-start | bytes 3145736 | tf_op jit(solution)/shard_map/ppermute | solution.py:459
  99.3 5.9 %collective-permute-done.11.refs_6_ = bf16[128,2048]{1,0:T(8,128)(2,1)} collective-permute-done((bf16[128,2048]{1,0:T(8,128)(2,1)}, bf16[128,2048]{1,0:T(8,128)(2,1)}, u32[]{:S(2)}, u32[]{:S(2)}) %collective-permute-start.11) | collective-permute-done | bytes 524320 | tf_op jit(solution)/shard_map/ppermute | solution.py:459
  105.1 1.7 collective-permute-done.12.refs_7_
  106.8 3.7 %collective-permute-start.13 = (bf16[128,2048]{1,0:T(8,128)(2,1)}, bf16[128,2048]{1,0:T(8,128)(2,1)S(1)}, u32[]{:S(2)}, u32[]{:S(2)}) collective-permute-start(bf16[128,2048]{1,0:T(8,128)(2,1)} %collective-permute-done.12.refs_7_), channel_id=1, source_target_pairs={{0,14},{1,3},{2,0},{3,5},{4,2},{5,7},{6,4},{7,9},{8,6},{9,11},{10,... | collective-permute-start | bytes 1572872 | tf_op jit(solution)/shard_map/ppermute | solution.py:459
  110.5 6.7 %experts.2.refs_10_ = bf16[512,2048]{1,0:T(8,128)(2,1)} custom-call(bf16[256,2048]{1,0:T(8,128)(2,1)} %bitcast.19, bf16[256,2048]{1,0:T(8,128)(2,1)} %collective-permute-done.7.refs_1_.x_ref, bf16[2,2048,128]{2,1,0:T(8,128)(2,1)} %constant_dynamic-update-slice_fusion.refs_2_, bf16[2,2048,128]{2,1,0:T(8,128)(2,1)} %collective-permute-done.1.refs_3_, ...), custom_call_target="tpu_custom_call" | custom-call | flops 2415919104 | bytes 6291456 | tf_op jit(solution)/shard_map/experts/pallas_call | solution.py:184
  117.2 2.8 %attend.3 = bf16[512,128]{1,0:T(8,128)(2,1)} custom-call(s32[1]{0:T(128)} %bitcast.ep_ref, f32[1,128]{1,0:T(1,128)S(1)} %broadcast_in_dim.15.base_ref, bf16[1024,128]{1,0:T(8,128)(2,1)S(1)} %widen.1.q_ref, bf16[16,1056,128]{2,1,0:T(8,128)(2,1)} %bitcast.23, f32[1024,128]{1,0:T(8,128)S(1)} %get-tuple-element.34.rest_0_, f32[1024,128]{1,0:T(8,128)S(1)} %get-tuple-element.35.rest_1_), custom_call_target="tpu_custom_call" | custom-call | flops 8589934592 | bytes 4194304 | tf_op jit(solution)/shard_map/attend/pallas_call | solution.py:361
  120.0 7.5 %collective-permute-done.5.refs_4_ = bf16[2,2048,128]{2,1,0:T(8,128)(2,1)S(1)} collective-permute-done((bf16[2,2048,128]{2,1,0:T(8,128)(2,1)}, bf16[2,2048,128]{2,1,0:T(8,128)(2,1)S(1)}, u32[]{:S(2)}, u32[]{:S(2)}) %collective-permute-start.5) | collective-permute-done | bytes 1048608 | tf_op jit(solution)/shard_map/ppermute | solution.py:459
  128.5 2.0 collective-permute-start.15
  130.5 5.5 %collective-permute-done.13.refs_9_ = bf16[128,2048]{1,0:T(8,128)(2,1)S(1)} collective-permute-done((bf16[128,2048]{1,0:T(8,128)(2,1)}, bf16[128,2048]{1,0:T(8,128)(2,1)S(1)}, u32[]{:S(2)}, u32[]{:S(2)}) %collective-permute-start.13) | collective-permute-done | bytes 524320 | tf_op jit(solution)/shard_map/ppermute | solution.py:459
  136.0 3.6 %collective-permute-start.14 = (bf16[128,2048]{1,0:T(8,128)(2,1)S(1)}, bf16[128,2048]{1,0:T(8,128)(2,1)S(1)}, u32[]{:S(2)}, u32[]{:S(2)}) collective-permute-start(bf16[128,2048]{1,0:T(8,128)(2,1)S(1)} %collective-permute-done.13.refs_9_), channel_id=1, source_target_pairs={{0,14},{1,3},{2,0},{3,5},{4,2},{5,7},{6,4},{7,9},{8,6},{9,11},{10,... | collective-permute-start | bytes 1572872 | tf_op jit(solution)/shard_map/ppermute | solution.py:511
  139.6 18.1 %collective-permute-done.15.refs_8_ = bf16[128,2048]{1,0:T(8,128)(2,1)S(1)} collective-permute-done((bf16[128,2048]{1,0:T(8,128)(2,1)}, bf16[128,2048]{1,0:T(8,128)(2,1)S(1)}, u32[]{:S(2)}, u32[]{:S(2)}) %collective-permute-start.15) | collective-permute-done | bytes 524320 | tf_op jit(solution)/shard_map/ppermute | solution.py:459
  158.5 7.5 %experts.3.y_ref = bf16[512,2048]{1,0:T(8,128)(2,1)} custom-call(bf16[256,2048]{1,0:T(8,128)(2,1)} %bitcast.20, bf16[256,2048]{1,0:T(8,128)(2,1)} %collective-permute-done.7.refs_1_.x_ref, bf16[2,2048,128]{2,1,0:T(8,128)(2,1)} %collective-permute-done.3.refs_2_, bf16[2,2048,128]{2,1,0:T(8,128)(2,1)} %collective-permute-done.4.refs_3_, ...), custom_call_target="tpu_custom_call" | custom-call | flops 3221225472 | bytes 6291456 | tf_op jit(solution)/shard_map/experts/pallas_call | solution.py:184
  166.1 2.8 %experts_last.3 = bf16[256,2048]{1,0:T(8,128)(2,1)S(1)} custom-call(bf16[256,2048]{1,0:T(8,128)(2,1)} %collective-permute-done.7.refs_1_.x_ref, bf16[2,2048,128]{2,1,0:T(8,128)(2,1)S(1)} %collective-permute-done.10.gu_ref, bf16[128,2048]{1,0:T(8,128)(2,1)S(1)} %collective-permute-done.14.d_ref, bf16[512,2048]{1,0:T(8,128)(2,1)} %experts.3.y_ref), custom_call_target="tpu_custom_call" | custom-call | flops 402653184 | bytes 5242880 | tf_op jit(solution)/shard_map/experts_last/pallas_call | solution.py:221
  169.0 5.5 %all-to-all-start = ((bf16[16,32,128]{2,1,0:T(8,128)(2,1)}), bf16[16,32,128]{2,1,0:T(8,128)(2,1)S(1)}, u32[]{:S(2)}, u32[]{:S(2)}) async-start(bf16[16,32,128]{2,1,0:T(8,128)(2,1)} %bitcast.4), calls=%async_computation | async-start | bytes 262144 | tf_op jit(solution)/shard_map/all_to_all | solution.py:513
  174.5 2.8 %experts_last.2 = bf16[256,2048]{1,0:T(8,128)(2,1)S(1)} custom-call(bf16[256,2048]{1,0:T(8,128)(2,1)} %bitcast.21, bf16[2,2048,128]{2,1,0:T(8,128)(2,1)S(1)} %collective-permute-done.10.gu_ref, bf16[128,2048]{1,0:T(8,128)(2,1)S(1)} %collective-permute-done.14.d_ref, bf16[512,2048]{1,0:T(8,128)(2,1)} %experts.3.y_ref), custom_call_target="tpu_custom_call" | custom-call | flops 402653184 | bytes 5242880 | tf_op jit(solution)/shard_map/experts_last/pallas_call | solution.py:221
  177.4 2.6 %add_convert_fusion = bf16[256,2048]{1,0:T(8,128)(2,1)} fusion(bf16[256,2048]{1,0:T(8,128)(2,1)} %collective-permute-done.16, bf16[256,2048]{1,0:T(8,128)(2,1)S(1)} %experts_last.2), kind=kLoop, calls=%fused_computation | loop fusion | flops 2097152 | bytes 3145728 | tf_op jit(solution)/shard_map/convert_element_type | solution.py:526
  180.0 3.2 %all-to-all-done.a_ref = bf16[16,32,128]{2,1,0:T(8,128)(2,1)S(1)} async-done(((bf16[16,32,128]{2,1,0:T(8,128)(2,1)}), bf16[16,32,128]{2,1,0:T(8,128)(2,1)S(1)}, u32[]{:S(2)}, u32[]{:S(2)}) %all-to-all-start) | async-done | bytes 131104 | tf_op jit(solution)/shard_map/all_to_all | solution.py:513
  183.2 10.9 %all-to-all-start.2 = ((bf16[16,16,2048]{2,1,0:T(8,128)(2,1)}), bf16[16,16,2048]{2,1,0:T(8,128)(2,1)S(1)}, u32[]{:S(2)}, u32[]{:S(2)}) async-start(bf16[16,16,2048]{2,1,0:T(8,128)(2,1)} %bitcast.9), calls=%async_computation.2 | async-start | bytes 2097152 | tf_op jit(solution)/shard_map/all_to_all | solution.py:527
  194.7 2.2 copy-done.1
  196.9 3.6 %project.1 = bf16[64,2048]{1,0:T(8,128)(2,1)} custom-call(bf16[16,32,128]{2,1,0:T(8,128)(2,1)S(1)} %all-to-all-done.a_ref, bf16[16,1024,128]{2,1,0:T(8,128)(2,1)S(1)} %bitcast.15), custom_call_target="tpu_custom_call" | custom-call | tf_op jit(solution)/shard_map/project/pallas_call | solution.py:422
  200.5 10.3 %all-to-all-done.2 = bf16[16,16,2048]{2,1,0:T(8,128)(2,1)S(1)} async-done(((bf16[16,16,2048]{2,1,0:T(8,128)(2,1)}), bf16[16,16,2048]{2,1,0:T(8,128)(2,1)S(1)}, u32[]{:S(2)}, u32[]{:S(2)}) %all-to-all-start.2) | async-done | bytes 1048608 | tf_op jit(solution)/shard_map/all_to_all | solution.py:527
  210.8 1.2 combine.1
  (66 shorter events, 9.1 us)
Async XLA Ops:
  7.2 4.2 %copy-start = (bf16[64,2048]{1,0:T(8,128)(2,1)S(1)}, bf16[64,2048]{1,0:T(8,128)(2,1)}, u32[]{:S(2)}) copy-start(bf16[64,2048]{1,0:T(8,128)(2,1)} %param.16) | copy-start | bytes 786436
  7.2 24.7 %copy-start.9 = (bf16[1,2048,128]{2,1,0:T(8,128)(2,1)S(1)}, bf16[1,2048,128]{2,1,0:T(8,128)(2,1)}, u32[]{:S(2)}) copy-start(bf16[1,2048,128]{2,1,0:T(8,128)(2,1)} %param.19) | copy-start | bytes 1572868
  7.2 72.6 %all-gather.5.cloned.1.call-start = ((), (), s32[]{:S(2)}) async-start(), calls=%async_computation.3 | async-start | bytes 4595712 | tf_op jit(solution)/shard_map/all_gather | solution.py:476
  8.2 24.6 %copy-start.10 = (bf16[1,2048,128]{2,1,0:T(8,128)(2,1)S(1)}, bf16[1,2048,128]{2,1,0:T(8,128)(2,1)}, u32[]{:S(2)}) copy-start(bf16[1,2048,128]{2,1,0:T(8,128)(2,1)} %param.20) | copy-start | bytes 1572868
  10.4 27.6 %copy-start.12 = (s32[96,2]{0,1:T(2,128)S(1)}, s32[96,2]{0,1:T(2,128)}, u32[]{:S(2)}) copy-start(s32[96,2]{0,1:T(2,128)} %param.22) | copy-start | bytes 2308
  10.4 27.7 %copy-start.2 = (bf16[96,2048]{1,0:T(8,128)(2,1)S(1)}, bf16[96,2048]{1,0:T(8,128)(2,1)}, u32[]{:S(2)}) copy-start(bf16[96,2048]{1,0:T(8,128)(2,1)} %tokens_ref.1) | copy-start | bytes 1179652
  10.4 27.7 %copy-start.3 = (f32[2048]{0:T(1024)S(1)}, f32[2048]{0:T(1024)}, u32[]{:S(2)}) copy-start(f32[2048]{0:T(1024)} %param.18) | copy-start | bytes 24580
  11.3 183.4 %all-gather.7.cloned.1.call-start = ((), (), s32[]{:S(2)}) async-start(), calls=%async_computation.4 | async-start | bytes 4456448 | tf_op jit(solution)/shard_map/all_gather | solution.py:498
  11.4 3.8 %collective-permute-start = (bf16[64,128]{1,0:T(8,128)(2,1)S(1)}, bf16[64,128]{1,0:T(8,128)(2,1)S(1)}, u32[]{:S(2)}, u32[]{:S(2)}) collective-permute-start(bf16[64,128]{1,0:T(8,128)(2,1)S(1)} %constant_dynamic-slice_fusion), channel_id=1, source_target_pairs={{0,2},{1,3},{2,0},{3,1},{4,6},{5,7},{6,4},{7,5},{8,10},{9,11},{10,... | collective-permute-start | bytes 49160 | tf_op jit(solution)/shard_map/ppermute | solution.py:462
  15.2 5.2 %collective-permute-start.17 = (bf16[128,128]{1,0:T(8,128)(2,1)S(1)}, bf16[128,128]{1,0:T(8,128)(2,1)S(1)}, u32[]{:S(2)}, u32[]{:S(2)}) collective-permute-start(bf16[128,128]{1,0:T(8,128)(2,1)S(1)} %pad_maximum_fusion.2), channel_id=1, source_target_pairs={{0,4},{1,5},{2,6},{3,7},{4,0},{5,1},{6,2},{7,3},{8,12},{9,13},{10,... | collective-permute-start | bytes 98312 | tf_op jit(solution)/shard_map/ppermute | solution.py:462
  20.4 9.3 %collective-permute-start.18 = (bf16[256,128]{1,0:T(8,128)(2,1)S(1)}, bf16[256,128]{1,0:T(8,128)(2,1)S(1)}, u32[]{:S(2)}, u32[]{:S(2)}) collective-permute-start(bf16[256,128]{1,0:T(8,128)(2,1)S(1)} %constant_dynamic-update-slice_fusion.2.low_ref), channel_id=1, source_target_pairs={{0,8},{1,9},{2,10},{3,11},{4,12},{5,13},{6,14},{7,15},{8,0},{9,1},... | collective-permute-start | bytes 196616 | tf_op jit(solution)/shard_map/ppermute | solution.py:462
  29.7 1.4 collective-permute-start.19
  32.7 14.7 %copy-start.14 = (bf16[1,128,2048]{2,1,0:T(8,128)(2,1)S(1)}, bf16[1,128,2048]{2,1,0:T(8,128)(2,1)}, u32[]{:S(2)}) copy-start(bf16[1,128,2048]{2,1,0:T(8,128)(2,1)} %param.21) | copy-start | bytes 1572868
  32.7 19.2 %copy-start.11 = (bf16[1024,64]{0,1:T(8,128)(2,1)S(1)}, bf16[1024,64]{0,1:T(8,128)(2,1)}, u32[]{:S(2)}) copy-start(bf16[1024,64]{0,1:T(8,128)(2,1)} %param.12) | copy-start | bytes 393220
  33.6 26.6 %collective-permute-start.1 = (bf16[2,2048,128]{2,1,0:T(8,128)(2,1)}, bf16[2,2048,128]{2,1,0:T(8,128)(2,1)}, u32[]{:S(2)}, u32[]{:S(2)}) collective-permute-start(bf16[2,2048,128]{2,1,0:T(8,128)(2,1)} %constant_dynamic-update-slice_fusion.refs_2_), channel_id=1, source_target_pairs={{0,2},{1,15},{2,4},{3,1},{4,6},{5,3},{6,8},{7,5},{8,10},{9,7},{10,... | collective-permute-start | bytes 3145736 | tf_op jit(solution)/shard_map/ppermute | solution.py:459
  34.4 27.5 %collective-permute-start.2 = (bf16[2,2048,128]{2,1,0:T(8,128)(2,1)}, bf16[2,2048,128]{2,1,0:T(8,128)(2,1)}, u32[]{:S(2)}, u32[]{:S(2)}) collective-permute-start(bf16[2,2048,128]{2,1,0:T(8,128)(2,1)} %constant_dynamic-update-slice_fusion.refs_2_), channel_id=1, source_target_pairs={{0,14},{1,3},{2,0},{3,5},{4,2},{5,7},{6,4},{7,9},{8,6},{9,11},{10,... | collective-permute-start | bytes 3145736 | tf_op jit(solution)/shard_map/ppermute | solution.py:459
  39.9 32.7 %all-to-all-start.1 = ((bf16[16,16,2048]{2,1,0:T(8,128)(2,1)}), bf16[16,16,2048]{2,1,0:T(8,128)(2,1)S(1)}, u32[]{:S(2)}, u32[]{:S(2)}) async-start(bf16[16,16,2048]{2,1,0:T(8,128)(2,1)} %bitcast.6), calls=%async_computation.1 | async-start | bytes 2097152 | tf_op jit(solution)/shard_map/all_to_all | solution.py:484
  47.4 25.2 %collective-permute-start.8 = (bf16[128,2048]{1,0:T(8,128)(2,1)S(1)}, bf16[128,2048]{1,0:T(8,128)(2,1)}, u32[]{:S(2)}, u32[]{:S(2)}) collective-permute-start(bf16[128,2048]{1,0:T(8,128)(2,1)S(1)} %bitcast.25), channel_id=1, source_target_pairs={{0,2},{1,15},{2,4},{3,1},{4,6},{5,3},{6,8},{7,5},{8,10},{9,7},{10,... | collective-permute-start | bytes 1572872 | tf_op jit(solution)/shard_map/ppermute | solution.py:459
  47.5 25.5 %collective-permute-start.9 = (bf16[128,2048]{1,0:T(8,128)(2,1)S(1)}, bf16[128,2048]{1,0:T(8,128)(2,1)}, u32[]{:S(2)}, u32[]{:S(2)}) collective-permute-start(bf16[128,2048]{1,0:T(8,128)(2,1)S(1)} %bitcast.26), channel_id=1, source_target_pairs={{0,14},{1,3},{2,0},{3,5},{4,2},{5,7},{6,4},{7,9},{8,6},{9,11},{10,... | collective-permute-start | bytes 1572872 | tf_op jit(solution)/shard_map/ppermute | solution.py:459
  62.5 31.4 %collective-permute-start.3 = (bf16[2,2048,128]{2,1,0:T(8,128)(2,1)}, bf16[2,2048,128]{2,1,0:T(8,128)(2,1)}, u32[]{:S(2)}, u32[]{:S(2)}) collective-permute-start(bf16[2,2048,128]{2,1,0:T(8,128)(2,1)} %collective-permute-done.1.refs_3_), channel_id=1, source_target_pairs={{0,2},{1,15},{2,4},{3,1},{4,6},{5,3},{6,8},{7,5},{8,10},{9,7},{10,... | collective-permute-start | bytes 3145736 | tf_op jit(solution)/shard_map/ppermute | solution.py:459
  63.8 31.7 %collective-permute-start.4 = (bf16[2,2048,128]{2,1,0:T(8,128)(2,1)}, bf16[2,2048,128]{2,1,0:T(8,128)(2,1)}, u32[]{:S(2)}, u32[]{:S(2)}) collective-permute-start(bf16[2,2048,128]{2,1,0:T(8,128)(2,1)} %collective-permute-done.2.refs_4_), channel_id=1, source_target_pairs={{0,14},{1,3},{2,0},{3,5},{4,2},{5,7},{6,4},{7,9},{8,6},{9,11},{10,... | collective-permute-start | bytes 3145736 | tf_op jit(solution)/shard_map/ppermute | solution.py:459
  72.6 12.0 %copy-start.4 = (bf16[16,16,2048]{2,1,0:T(8,128)(2,1)}, bf16[16,16,2048]{2,1,0:T(8,128)(2,1)S(1)}, u32[]{:S(2)}) copy-start(bf16[16,16,2048]{2,1,0:T(8,128)(2,1)S(1)} %all-to-all-done.1) | copy-start | bytes 3145732
  72.6 37.9 %collective-permute-start.7 = (bf16[256,2048]{1,0:T(8,128)(2,1)S(1)}, bf16[256,2048]{1,0:T(8,128)(2,1)}, u32[]{:S(2)}, u32[]{:S(2)}) collective-permute-start(bf16[256,2048]{1,0:T(8,128)(2,1)S(1)} %bitcast.18), channel_id=1, source_target_pairs={{0,1},{1,0},{2,3},{3,2},{4,5},{5,4},{6,7},{7,6},{8,9},{9,8},{10,11... | collective-permute-start | bytes 3145736 | tf_op jit(solution)/shard_map/ppermute | solution.py:500
  73.0 32.1 %collective-permute-start.11 = (bf16[128,2048]{1,0:T(8,128)(2,1)}, bf16[128,2048]{1,0:T(8,128)(2,1)}, u32[]{:S(2)}, u32[]{:S(2)}) collective-permute-start(bf16[128,2048]{1,0:T(8,128)(2,1)} %collective-permute-done.8.refs_6_), channel_id=1, source_target_pairs={{0,2},{1,15},{2,4},{3,1},{4,6},{5,3},{6,8},{7,5},{8,10},{9,7},{10,... | collective-permute-start | bytes 1572872 | tf_op jit(solution)/shard_map/ppermute | solution.py:459
  74.3 32.5 %collective-permute-start.12 = (bf16[128,2048]{1,0:T(8,128)(2,1)}, bf16[128,2048]{1,0:T(8,128)(2,1)}, u32[]{:S(2)}, u32[]{:S(2)}) collective-permute-start(bf16[128,2048]{1,0:T(8,128)(2,1)} %collective-permute-done.9.refs_7_), channel_id=1, source_target_pairs={{0,14},{1,3},{2,0},{3,5},{4,2},{5,7},{6,4},{7,9},{8,6},{9,11},{10,... | collective-permute-start | bytes 1572872 | tf_op jit(solution)/shard_map/ppermute | solution.py:459
  95.6 31.9 %collective-permute-start.5 = (bf16[2,2048,128]{2,1,0:T(8,128)(2,1)}, bf16[2,2048,128]{2,1,0:T(8,128)(2,1)S(1)}, u32[]{:S(2)}, u32[]{:S(2)}) collective-permute-start(bf16[2,2048,128]{2,1,0:T(8,128)(2,1)} %collective-permute-done.3.refs_2_), channel_id=1, source_target_pairs={{0,2},{1,15},{2,4},{3,1},{4,6},{5,3},{6,8},{7,5},{8,10},{9,7},{10,... | collective-permute-start | bytes 3145736 | tf_op jit(solution)/shard_map/ppermute | solution.py:459
  96.8 31.6 %collective-permute-start.6 = (bf16[2,2048,128]{2,1,0:T(8,128)(2,1)}, bf16[2,2048,128]{2,1,0:T(8,128)(2,1)S(1)}, u32[]{:S(2)}, u32[]{:S(2)}) collective-permute-start(bf16[2,2048,128]{2,1,0:T(8,128)(2,1)} %collective-permute-done.4.refs_3_), channel_id=1, source_target_pairs={{0,14},{1,3},{2,0},{3,5},{4,2},{5,7},{6,4},{7,9},{8,6},{9,11},{10,... | collective-permute-start | bytes 3145736 | tf_op jit(solution)/shard_map/ppermute | solution.py:459
  106.8 29.2 %collective-permute-start.13 = (bf16[128,2048]{1,0:T(8,128)(2,1)}, bf16[128,2048]{1,0:T(8,128)(2,1)S(1)}, u32[]{:S(2)}, u32[]{:S(2)}) collective-permute-start(bf16[128,2048]{1,0:T(8,128)(2,1)} %collective-permute-done.12.refs_7_), channel_id=1, source_target_pairs={{0,14},{1,3},{2,0},{3,5},{4,2},{5,7},{6,4},{7,9},{8,6},{9,11},{10,... | collective-permute-start | bytes 1572872 | tf_op jit(solution)/shard_map/ppermute | solution.py:459
  127.5 30.2 %copy-start.5 = (bf16[2,2048,128]{2,1,0:T(8,128)(2,1)}, bf16[2,2048,128]{2,1,0:T(8,128)(2,1)S(1)}, u32[]{:S(2)}) copy-start(bf16[2,2048,128]{2,1,0:T(8,128)(2,1)S(1)} %collective-permute-done.5.refs_4_) | copy-start | bytes 3145732
  128.4 29.3 %copy-start.6 = (bf16[2,2048,128]{2,1,0:T(8,128)(2,1)}, bf16[2,2048,128]{2,1,0:T(8,128)(2,1)S(1)}, u32[]{:S(2)}) copy-start(bf16[2,2048,128]{2,1,0:T(8,128)(2,1)S(1)} %collective-permute-done.6.refs_5_) | copy-start | bytes 3145732
  128.4 37.6 %collective-permute-start.10 = (bf16[2,2048,128]{2,1,0:T(8,128)(2,1)S(1)}, bf16[2,2048,128]{2,1,0:T(8,128)(2,1)S(1)}, u32[]{:S(2)}, u32[]{:S(2)}) collective-permute-start(bf16[2,2048,128]{2,1,0:T(8,128)(2,1)S(1)} %collective-permute-done.5.refs_4_), channel_id=1, source_target_pairs={{0,2},{1,15},{2,4},{3,1},{4,6},{5,3},{6,8},{7,5},{8,10},{9,7},{10,... | collective-permute-start | bytes 3145736 | tf_op jit(solution)/shard_map/ppermute | solution.py:519
  128.5 29.3 %collective-permute-start.15 = (bf16[128,2048]{1,0:T(8,128)(2,1)}, bf16[128,2048]{1,0:T(8,128)(2,1)S(1)}, u32[]{:S(2)}, u32[]{:S(2)}) collective-permute-start(bf16[128,2048]{1,0:T(8,128)(2,1)} %collective-permute-done.11.refs_6_), channel_id=1, source_target_pairs={{0,2},{1,15},{2,4},{3,1},{4,6},{5,3},{6,8},{7,5},{8,10},{9,7},{10,... | collective-permute-start | bytes 1572872 | tf_op jit(solution)/shard_map/ppermute | solution.py:459
  136.0 21.7 %copy-start.7 = (bf16[128,2048]{1,0:T(8,128)(2,1)}, bf16[128,2048]{1,0:T(8,128)(2,1)S(1)}, u32[]{:S(2)}) copy-start(bf16[128,2048]{1,0:T(8,128)(2,1)S(1)} %collective-permute-done.13.refs_9_) | copy-start | bytes 1572868
  136.0 30.0 %collective-permute-start.14 = (bf16[128,2048]{1,0:T(8,128)(2,1)S(1)}, bf16[128,2048]{1,0:T(8,128)(2,1)S(1)}, u32[]{:S(2)}, u32[]{:S(2)}) collective-permute-start(bf16[128,2048]{1,0:T(8,128)(2,1)S(1)} %collective-permute-done.13.refs_9_), channel_id=1, source_target_pairs={{0,14},{1,3},{2,0},{3,5},{4,2},{5,7},{6,4},{7,9},{8,6},{9,11},{10,... | collective-permute-start | bytes 1572872 | tf_op jit(solution)/shard_map/ppermute | solution.py:511
  157.7 0.8 copy-start.8
  168.9 8.5 %collective-permute-start.16 = (bf16[256,2048]{1,0:T(8,128)(2,1)S(1)}, bf16[256,2048]{1,0:T(8,128)(2,1)}, u32[]{:S(2)}, u32[]{:S(2)}) collective-permute-start(bf16[256,2048]{1,0:T(8,128)(2,1)S(1)} %experts_last.3), channel_id=1, source_target_pairs={{0,1},{1,0},{2,3},{3,2},{4,5},{5,4},{6,7},{7,6},{8,9},{9,8},{10,11... | collective-permute-start | bytes 3145736 | tf_op jit(solution)/shard_map/ppermute | solution.py:524
  169.0 14.2 %all-to-all-start = ((bf16[16,32,128]{2,1,0:T(8,128)(2,1)}), bf16[16,32,128]{2,1,0:T(8,128)(2,1)S(1)}, u32[]{:S(2)}, u32[]{:S(2)}) async-start(bf16[16,32,128]{2,1,0:T(8,128)(2,1)} %bitcast.4), calls=%async_computation | async-start | bytes 262144 | tf_op jit(solution)/shard_map/all_to_all | solution.py:513
  177.4 16.8 %copy-start.13 = (f32[96,2]{0,1:T(2,128)S(1)}, f32[96,2]{0,1:T(2,128)}, u32[]{:S(2)}) copy-start(f32[96,2]{0,1:T(2,128)} %param.23) | copy-start | bytes 2308
  183.2 27.6 %all-to-all-start.2 = ((bf16[16,16,2048]{2,1,0:T(8,128)(2,1)}), bf16[16,16,2048]{2,1,0:T(8,128)(2,1)S(1)}, u32[]{:S(2)}, u32[]{:S(2)}) async-start(bf16[16,16,2048]{2,1,0:T(8,128)(2,1)} %bitcast.9), calls=%async_computation.2 | async-start | bytes 2097152 | tf_op jit(solution)/shard_map/all_to_all | solution.py:527
  194.7 2.2 %copy-start.1 = (bf16[16384,128]{1,0:T(8,128)(2,1)S(1)}, bf16[16384,128]{1,0:T(8,128)(2,1)}, u32[]{:S(2)}) copy-start(bf16[16384,128]{1,0:T(8,128)(2,1)} %all-gather.7.cloned.1.call-done) | copy-start | bytes 12582916
Sparse Core Ops, SparseCore 0:
  11.4 68.2 all-gather.4
  82.7 53.5 all-gather.6
